TPU v7x, 256 devices: a whole 4x4x8 slice. The times are simulated.
256 devices in a mesh: sp: 32 (over z, x), tp: 8 (over y, core).
Axes of the slice: x: 4, y: 4, z: 8, core: 2. Of those that a mesh axis runs over, the one named last changes fastest.
Arguments:
- tokens: bfloat16 [8192, 1024], P(('sp', 'tp')), may hold values from -6 to 6
- doc_ids: int32 [8192], P('sp'), may hold values from 0 to 31, never falling along the last dimension, each value on 1 to 4608 neighbouring positions
- down_query: bfloat16 [1024, 256], P('sp'), may hold values from -0.1875 to 0.1875
- down_key: bfloat16 [1024, 256], P('sp'), may hold values from -0.1875 to 0.1875
- down_rotary: bfloat16 [1024, 32], P('sp'), may hold values from -0.1875 to 0.1875
- query_gain: float32 [256], replicated, may hold values from 0.1 to 1.9
- key_gain: float32 [256], replicated, may hold values from 0.1 to 1.9
- up_query: bfloat16 [256, 1536], P('sp', 'tp'), may hold values from -0.375 to 0.375
- up_key: bfloat16 [256, 1024], P('sp', 'tp'), may hold values from -0.375 to 0.375
- up_value: bfloat16 [256, 1024], P('sp', 'tp'), may hold values from -0.375 to 0.375
- output_weight: bfloat16 [1024, 1024], P('tp', 'sp'), may hold values from -0.1875 to 0.1875
- out_gain: float32 [1024], replicated, may hold values from 0.1 to 1.9
Outputs:
- mixed: bfloat16 [8192, 1024], P(('sp', 'tp'))
- log_sums: float32 [8192, 16], P('sp', 'tp')
Inputs may be any that keep to these rules, and one draw needn't show every extreme that they name: doc_ids never fall along the sequence and run from 0 to at most the number of devices along sp minus one; each document has 1 to 4608 positions, and one document has exactly that many.
All inputs are finite; a program needn't handle non-finite values.
Results may differ from a plain program's by a relative error of at most 0.02.
Values may be sent and summed in bfloat16 or wider, within the bound.
A program may use at most 64 MiB of HBM per device.

v0:
```python
import functools
import math

import jax
import jax.numpy as jnp
import numpy as np
from jax import lax
from jax.experimental import pallas as pl
from jax.experimental.pallas import tpu as pltpu
from jax.sharding import PartitionSpec as P

NOPE = 64
ROPE = 32
VDIM = 64
THETA = 10000.0
EPS = 1e-06
MASKED = -1e30
MESH = pl.DeviceIdType.MESH
F32 = jnp.float32
BF16 = jnp.bfloat16


def dot(a, b):
    return jnp.dot(a, b, preferred_element_type=F32)


def rows_joined(blocks, flat):
    n, r, c = blocks.shape
    for j in range(n):
        flat[j * r : (j + 1) * r, :] = blocks[j]
    return flat


def rms_parts(parts, gains):
    wide = [part.astype(F32) for part in parts]
    width = sum(part.shape[-1] for part in parts)
    total = sum(jnp.sum(part * part, axis=-1, keepdims=True) for part in wide)
    scale = lax.rsqrt(total / width + EPS)
    return [(part * scale * gain).astype(BF16) for part, gain in zip(wide, gains)]


def tables(tokens, heads):
    half = ROPE // 2
    inverse = np.float32(THETA) ** (-np.arange(half, dtype=np.float32) / np.float32(half))
    angles = np.arange(tokens, dtype=np.float32)[:, None] * inverse.astype(np.float32)[None, :]
    turn = np.zeros((tokens, 256), np.float32)
    turn[:, :ROPE] = np.tile(np.cos(angles), (1, 2))
    turn[:, 128 : 128 + ROPE] = np.tile(np.sin(angles), (1, 2))
    width = NOPE + ROPE
    pick = np.zeros((heads * width, heads * 384), np.float32)
    eye = np.arange(NOPE)
    rot = np.arange(ROPE)
    for head in range(heads):
        pick[head * width + eye, head * 384 + (head % 2) * NOPE + eye] = 1
        pick[head * width + NOPE + rot, head * 384 + 128 + rot] = 1
        low = np.arange(half)
        pick[head * width + NOPE + half + low, head * 384 + 256 + low] = -1
        pick[head * width + NOPE + low, head * 384 + 256 + half + low] = 1
    pick_key = np.zeros((ROPE, 256), np.float32)
    pick_key[rot, rot] = 1
    pick_key[half + low, 128 + low] = -1
    pick_key[low, 128 + half + low] = 1
    return turn, pick, pick_key


def kernel(
    n, ntp, heads,
    tokens, docs, down_q, down_k, down_r, gain_q, gain_k, up_q, up_k, up_v, out_w, gain_o,
    turn, pick, pick_key,
    out, log_out,
    tok, wd, wr, uq, up, wo, qraw, kraw, krot, tab, sel, qs, values, scores, att, part, got_core, got_y, send_y, wd_flat, wr_flat, uq_flat, up_flat,
    loc, s_uq, r_uq, s_tok, r_tok, s_wd, r_wd, s_wr, r_wr, s_up, r_up, s_wo, r_wo,
    s_q, r_q, s_k, r_k, s_ky, r_ky, s_kc, r_kc, s_kr, r_kr, s_krc, r_krc, s_f, r_f,
):
    half = n // 2
    me = lax.axis_index("sp")
    t = lax.axis_index("tp")
    ny = ntp // 2
    y = t // 2
    yh = lax.rem(y, 2)
    core = lax.rem(t, 2)
    own = tokens.shape[0]
    block = ntp * own
    side = block // 2
    cols = wd.shape[-1]
    partner = me + 1 - 2 * lax.rem(me, 2)
    other_core = t + 1 - 2 * core
    other_y = (y + 1 - 2 * yh) * 2 + core

    def dev(sp, tp):
        return (sp, tp)

    x_dev = dev(partner, t)
    y_dev = dev(me, other_y)
    c_dev = dev(me, other_core)

    col = pl.multiple_of(yh * cols, cols)
    c_tok = pltpu.make_async_copy(tokens, tok.at[t], loc.at[0])
    c_wr = pltpu.make_async_copy(down_r, wr.at[me], loc.at[2])
    nq, nk = up_q.shape[1], up_k.shape[1]
    c_up = [
        pltpu.make_async_copy(up_q, uq.at[me], loc.at[3]),
        pltpu.make_async_copy(up_k, up.at[me, :, pl.ds(0, nk)], loc.at[4]),
        pltpu.make_async_copy(up_v, up.at[me, :, pl.ds(nk, nk)], loc.at[5]),
    ]
    c_wo = pltpu.make_async_copy(out_w, wo.at[me], loc.at[6])
    c_tab = pltpu.make_async_copy(turn.at[me], tab, loc.at[7])
    c_sel = pltpu.make_async_copy(pick, sel, loc.at[8])
    c_tok.start()

    @pl.when(core == 0)
    def _():
        pltpu.make_async_copy(down_k.at[:, pl.ds(col, cols)], wd.at[me], loc.at[1]).start()

    @pl.when(core == 1)
    def _():
        pltpu.make_async_copy(down_q.at[:, pl.ds(col, cols)], wd.at[me], loc.at[1]).start()

    c_wd = pltpu.make_async_copy(down_q.at[:, pl.ds(0, cols)], wd.at[me], loc.at[1])
    for copy in [c_wr] + c_up + [c_wo, c_tab, c_sel]:
        copy.start()

    barrier = pltpu.get_barrier_semaphore()
    for k in range(1, n):
        pl.semaphore_signal(barrier, inc=1, device_id=dev(lax.rem(me + k, n), t), device_id_type=MESH)
    for k in range(1, ntp):
        pl.semaphore_signal(barrier, inc=1, device_id=dev(me, lax.rem(t + k, ntp)), device_id_type=MESH)

    def rc(src, dst, s, r, device):
        return pltpu.make_async_remote_copy(
            src_ref=src, dst_ref=dst, send_sem=s, recv_sem=r, device_id=device, device_id_type=MESH
        )

    class Gather:
        def __init__(self, at, s, r):
            self.at, self.s, self.r = at, s, r

        def z(self, k):
            return rc(self.at(me), self.at(me), self.s.at[k], self.r.at[k], dev(lax.rem(me + 2 * k, n), t))

        def x(self, k):
            ref = self.at(lax.rem(me - 2 * k + n, n))
            return rc(ref, ref, self.s.at[half + k], self.r.at[half + k], x_dev)

        def start_z(self):
            for k in range(1, half):
                self.z(k).start()

        def from_z(self, k):
            ref = self.at(lax.rem(me - 2 * k + n, n))
            rc(ref, ref, self.s.at[k], self.r.at[k], x_dev).wait_recv()

        def from_x(self, k):
            ref = self.at(lax.rem(partner - 2 * k + n, n))
            rc(ref, ref, self.s.at[half + k], self.r.at[half + k], x_dev).wait_recv()

        def hand_on(self):
            for k in range(1, half):
                self.from_z(k)
                self.x(k).start()

        def rest(self):
            for k in range(half):
                self.from_x(k)

        def drain(self):
            for k in range(1, half):
                self.z(k).wait_send()
            for k in range(half):
                self.x(k).wait_send()

    g_wd = Gather(lambda i: wd.at[i], s_wd, r_wd)
    g_wr = Gather(lambda i: wr.at[i], s_wr, r_wr)
    g_uq = Gather(lambda i: uq.at[i], s_uq, r_uq)
    g_up = Gather(lambda i: up.at[i], s_up, r_up)
    g_wo = Gather(lambda i: wo.at[i], s_wo, r_wo)
    g_k = Gather(lambda i: kraw.at[i, yh], s_k, r_k)
    g_kr = Gather(lambda i: krot.at[i], s_kr, r_kr)

    c_wd.wait()
    c_wr.wait()
    c_tok.wait()
    pl.semaphore_wait(barrier, n - 1 + ntp - 1)

    def y_at(k):
        return lax.rem(y + k, ny) * 2 + core

    def tok_y(k):
        return rc(tok.at[t], tok.at[t], s_tok.at[k], r_tok.at[k], dev(me, y_at(k)))

    def tok_from(k):
        ref = tok.at[y_at(ny - k)]
        return rc(ref, ref, s_tok.at[k], r_tok.at[k], c_dev)

    def tok_c(k):
        ref = tok.at[y_at(ny - k)]
        return rc(ref, ref, s_tok.at[ny + k], r_tok.at[ny + k], c_dev)

    for k in range(1, ny):
        tok_y(k).start()
    g_wd.start_z()
    g_wd.x(0).start()

    @pl.when(core == 1)
    def _():
        g_wr.start_z()
        g_wr.x(0).start()

    tok_c(0).start()
    for copy in c_up:
        copy.wait()
    g_up.start_z()
    g_uq.start_z()
    g_wd.hand_on()

    @pl.when(core == 1)
    def _():
        g_wr.hand_on()

    g_up.x(0).start()
    g_uq.x(0).start()
    for k in range(1, ny):
        tok_from(k).wait_recv()
        tok_c(k).start()

    down = lax.broadcasted_iota(jnp.int32, (block, block), 0)
    across = lax.broadcasted_iota(jnp.int32, (block, block), 1)
    doc_row = jnp.broadcast_to(docs[...].astype(F32), (block, block))
    doc_col = jnp.sum(jnp.where(down == across, doc_row, 0.0), axis=-1, keepdims=True)
    lane = lax.broadcasted_iota(jnp.int32, (block, 128), 1)
    in_docs = (lane >= ROPE) & (lane < ROPE + n)
    same = doc_col == (lane - ROPE).astype(F32)
    key_docs = jnp.where(in_docs & same, 1.0, 0.0)
    query_docs = jnp.where(in_docs & jnp.logical_not(same), MASKED, 0.0)

    for k in range(ny):
        tok_c(k).wait_recv()
    g_wd.rest()
    block_tokens = tok[...].reshape(block, tok.shape[-1])
    raw = dot(block_tokens, rows_joined(wd, wd_flat)[...]).astype(BF16)
    c_tab.wait()

    q_y = rc(qraw.at[yh], qraw.at[yh], s_q.at[0], r_q.at[0], y_dev)
    q_c = rc(qraw.at[yh], qraw.at[yh], s_q.at[1], r_q.at[1], c_dev)
    q_f = rc(qraw.at[1 - yh], qraw.at[1 - yh], s_q.at[2], r_q.at[2], c_dev)

    def k_y(i, slot):
        return rc(kraw.at[i, yh], kraw.at[i, yh], s_ky.at[slot], r_ky.at[slot], y_dev)

    def k_from_y(i, slot):
        return rc(kraw.at[i, 1 - yh], kraw.at[i, 1 - yh], s_ky.at[slot], r_ky.at[slot], y_dev)

    def k_c(i, which, slot):
        ref = kraw.at[i, which]
        return rc(ref, ref, s_kc.at[slot], r_kc.at[slot], c_dev)

    def kr_c(i, slot):
        return rc(krot.at[i], krot.at[i], s_krc.at[slot], r_krc.at[slot], c_dev)

    def block_of(slot):
        if slot < half:
            return lax.rem(me - 2 * slot + n, n)
        return lax.rem(partner - 2 * (slot - half) + n, n)

    @pl.when(core == 0)
    def _():
        kraw[me, yh] = raw
        g_k.start_z()
        g_k.x(0).start()
        k_y(me, 0).start()
        k_c(me, yh, 0).start()

    @pl.when(core == 1)
    def _():
        qraw[yh] = raw
        q_y.start()
        q_c.start()
        g_wr.rest()
        rotary = dot(block_tokens, rows_joined(wr, wr_flat)[...]).astype(BF16)
        both = dot(rotary, pick_key[...])
        turned = both[:, :128] * tab[:, :128] + both[:, 128:] * tab[:, 128:] + key_docs
        packed = turned[:side] + pltpu.roll(turned[side:], 64, 1)
        krot[me] = packed.astype(BF16)
        g_kr.start_z()
        g_kr.x(0).start()
        kr_c(me, 0).start()
        q_y.wait_recv()
        q_f.start()

    g_up.hand_on()
    g_uq.hand_on()
    c_wo.wait()

    g_wo.start_z()

    @pl.when(core == 0)
    def _():
        for k in range(1, half):
            g_k.from_z(k)
            g_k.x(k).start()
            k_y(block_of(k), k).start()
            k_c(block_of(k), yh, k).start()

    @pl.when(core == 1)
    def _():
        for k in range(1, half):
            g_kr.from_z(k)
            g_kr.x(k).start()
            kr_c(block_of(k), k).start()

    g_wo.x(0).start()
    g_up.rest()
    g_uq.rest()

    @pl.when(core == 0)
    def _():
        q_c.wait_recv()
        q_f.wait_recv()

    c_sel.wait()
    gq = gain_q[...]
    lat = rms_parts([qraw[0], qraw[1]], [gq[:, :cols], gq[:, cols:]])
    rows_joined(up, up_flat)
    rows_joined(uq, uq_flat)
    projected = (dot(lat[0], uq_flat[:cols, :]) + dot(lat[1], uq_flat[cols:, :])).astype(BF16)
    for head in range(heads):
        laid = dot(projected, sel[:, head * 384 : (head + 1) * 384])
        turned = laid[:, 128:256] * tab[:, :128] + laid[:, 256:] * tab[:, 128:] + query_docs
        plain = laid[:, :128].astype(BF16)
        rows = pl.ds((head % 2) * block, block)
        qs[head // 2, 0, rows, :128] = plain
        qs[head // 2, 1, rows, :128] = plain
        qs[head // 2, 0, rows, 128:] = turned.astype(BF16)
        qs[head // 2, 1, rows, 128:] = pltpu.roll(turned, 64, 1).astype(BF16)

    gk = gain_k[...]
    for slot in range(n):
        i = block_of(slot)

        @pl.when(core == 0)
        def _(slot=slot, i=i):
            if slot >= half:
                g_k.from_x(slot - half)
                k_y(i, slot).start()
                k_c(i, yh, slot).start()
            k_from_y(i, slot).wait_recv()
            k_c(i, 1 - yh, n + slot).start()
            kr_c(i, slot).wait_recv()

        @pl.when(core == 1)
        def _(slot=slot, i=i):
            if slot >= half:
                g_kr.from_x(slot - half)
                kr_c(i, slot).start()
            k_c(i, yh, slot).wait_recv()
            k_c(i, 1 - yh, n + slot).wait_recv()

        if slot > 0 and slot < half:
            g_wo.from_z(slot)
            g_wo.x(slot).start()

        lat = rms_parts([kraw[i, 0], kraw[i, 1]], [gk[:, :cols], gk[:, cols:]])
        kv = (dot(lat[0], up_flat[:cols, :]) + dot(lat[1], up_flat[cols:, :])).astype(BF16)
        values[i] = kv[:, nk:]
        rot = krot[i]
        for pair in range(heads // 2):
            for s in range(2):
                keys = jnp.concatenate(
                    [kv[s * side : (s + 1) * side, pair * 128 : (pair + 1) * 128], rot], axis=1
                )
                scores[pair, i, :, s * side : (s + 1) * side] = lax.dot_general(
                    qs[pair, s], keys, (((1,), (1,)), ((), ())), preferred_element_type=F32
                )

    scale = 1.0 / math.sqrt(NOPE + ROPE)
    factor = scale * math.log2(math.e)
    head_lane = lax.broadcasted_iota(jnp.int32, (block, nk), 1) // VDIM
    attended = jnp.zeros((block, nk), F32)
    sums = []
    for head in range(heads):
        rows = pl.ds((head % 2) * block, block)
        top = scores[head // 2, 0, rows, :]
        for i in range(1, n):
            top = jnp.maximum(top, scores[head // 2, i, rows, :])
        top = jnp.max(top, axis=-1, keepdims=True)
        shift = top * factor
        total = jnp.zeros((block, block), F32)
        mixed = jnp.zeros((block, nk), F32)
        for i in range(n):
            weights = jnp.exp2(scores[head // 2, i, rows, :] * factor - shift)
            total = total + weights
            mixed = mixed + dot(weights.astype(BF16), values[i])
        weight_sum = jnp.sum(total, axis=-1, keepdims=True)
        attended = jnp.where(head_lane == head, mixed / weight_sum, attended)
        sums.append(top * scale + jnp.log(weight_sum))
    log_out[...] = jnp.concatenate(sums, axis=1)
    att[...] = attended.astype(BF16)

    g_wo.rest()

    def partial(owner):
        rows = att[pl.ds(pl.multiple_of(owner * own, own), own), :]
        return jnp.concatenate([dot(rows, wo[j]) for j in range(n)], axis=1)

    def f_c(k):
        return rc(part.at[k], got_core.at[k], s_f.at[k], r_f.at[k], c_dev)

    def f_y(k):
        return rc(send_y.at[k], got_y.at[k], s_f.at[ny + k], r_f.at[ny + k], dev(me, y_at(k)))

    order = list(range(1, ny)) + [0]
    for k in order:
        part[k] = partial(lax.rem(y + k, ny) * 2 + 1 - core).astype(BF16)
        f_c(k).start()
    for k in order[:-1]:
        far = partial(y_at(k))
        f_c(k).wait_recv()
        send_y[k] = (far + got_core[k].astype(F32)).astype(BF16)
        f_y(k).start()
    near = partial(t)
    f_c(0).wait_recv()
    near = near + got_core[0].astype(F32)
    for k in order[:-1]:
        f_y(k).wait_recv()
        near = near + got_y[k].astype(F32)
    out[...] = rms_parts([near.astype(BF16)], [gain_o[...]])[0]

    for k in range(ny):
        tok_c(k).wait_send()
        f_c(k).wait_send()
        if k > 0:
            tok_y(k).wait_send()
            f_y(k).wait_send()
    for gather in (g_wd, g_up, g_uq, g_wo):
        gather.drain()

    @pl.when(core == 0)
    def _():
        g_k.drain()
        for slot in range(n):
            k_y(block_of(slot), slot).wait_send()
            k_c(block_of(slot), yh, slot).wait_send()
            k_c(block_of(slot), 1 - yh, n + slot).wait_send()

    @pl.when(core == 1)
    def _():
        g_wr.drain()
        g_kr.drain()
        for slot in range(n):
            kr_c(block_of(slot), slot).wait_send()
        for copy in (q_y, q_c, q_f):
            copy.wait_send()


def on_device(n, ntp, tokens, doc_ids, down_q, down_k, down_r, gain_q, gain_k, up_q, up_k, up_v, out_w, gain_o):
    own, width = tokens.shape
    block = doc_ids.shape[0]
    heads = up_k.shape[1] // NOPE
    rank = down_k.shape[1]
    cols = rank // 2
    nq, nk, nv = up_q.shape[1], up_k.shape[1], up_v.shape[1]
    turn, pick, pick_key = tables(n * block, heads)
    turn = jnp.asarray(turn.reshape(n, block, 256))
    vmem = pl.BlockSpec(memory_space=pltpu.VMEM)
    hbm = pl.BlockSpec(memory_space=pl.ANY)
    dma = lambda k: pltpu.SemaphoreType.DMA((k,))
    scratch = [
        pltpu.VMEM((ntp, own, width), BF16),
        pltpu.VMEM((n, width // n, cols), BF16),
        pltpu.VMEM((n, width // n, down_r.shape[1]), BF16),
        pltpu.VMEM((n, up_q.shape[0], nq), BF16),
        pltpu.VMEM((n, up_q.shape[0], nk + nv), BF16),
        pltpu.VMEM((n,) + out_w.shape, BF16),
        pltpu.VMEM((2, block, cols), BF16),
        pltpu.VMEM((n, 2, block, cols), BF16),
        pltpu.VMEM((n, block // 2, 128), BF16),
        pltpu.VMEM((block, 256), F32),
        pltpu.VMEM(pick.shape, BF16),
        pltpu.VMEM((heads // 2, 2, 2 * block, 256), BF16),
        pltpu.VMEM((n, block, nv), BF16),
        pltpu.VMEM((heads // 2, n, 2 * block, block), F32),
        pltpu.VMEM((block, nv), BF16),
        pltpu.VMEM((ntp // 2, own, width), BF16),
        pltpu.VMEM((ntp // 2, own, width), BF16),
        pltpu.VMEM((ntp // 2, own, width), BF16),
        pltpu.VMEM((ntp // 2, own, width), BF16),
        pltpu.VMEM((width, cols), BF16),
        pltpu.VMEM((width, down_r.shape[1]), BF16),
        pltpu.VMEM((rank, nq), BF16),
        pltpu.VMEM((rank, nk + nv), BF16),
        dma(9), dma(n), dma(n), dma(ntp), dma(ntp),
        dma(n), dma(n), dma(n), dma(n), dma(n), dma(n), dma(n), dma(n),
        dma(3), dma(3), dma(n), dma(n), dma(n), dma(n),
        dma(2 * n), dma(2 * n), dma(n), dma(n), dma(n), dma(n), dma(ntp), dma(ntp),
    ]
    return pl.pallas_call(
        functools.partial(kernel, n, ntp, heads),
        out_shape=(
            jax.ShapeDtypeStruct((own, width), BF16),
            jax.ShapeDtypeStruct((block, heads), F32),
        ),
        in_specs=[hbm, vmem, hbm, hbm, hbm, vmem, vmem, hbm, hbm, hbm, hbm, vmem, hbm, hbm, vmem],
        out_specs=(vmem, vmem),
        scratch_shapes=scratch,
        compiler_params=pltpu.CompilerParams(
            collective_id=0, has_side_effects=True, vmem_limit_bytes=60 * 1024 * 1024
        ),
    )(
        tokens, doc_ids[None, :], down_q, down_k, down_r, gain_q[None, :], gain_k[None, :],
        up_q, up_k, up_v, out_w, gain_o[None, :],
        turn, jnp.asarray(pick, BF16), jnp.asarray(pick_key, BF16),
    )


def solution(mesh):
    assert mesh.shape["tp"] % 4 == 0 and mesh.shape["sp"] % 2 == 0 and mesh.shape["sp"] <= 32
    placed = (
        P(("sp", "tp"), None), P("sp"), P("sp", None), P("sp", None), P("sp", None), P(), P(),
        P("sp", "tp"), P("sp", "tp"), P("sp", "tp"), P("tp", "sp"), P(),
    )
    return jax.shard_map(
        functools.partial(on_device, mesh.shape["sp"], mesh.shape["tp"]),
        mesh=mesh,
        in_specs=placed,
        out_specs=(P(("sp", "tp"), None), P("sp", "tp")),
        check_vma=False,
    )
```

profile of v0, /device:TPU:1, one launch (start us, length us, event | category | flops | bytes accessed | tf_op | source)
XLA Modules:
  0.0 154.4 jit_solution(6303419449131296518)
XLA Ops:
  0.6 1.4 copy.17.out_w
  2.0 149.3 %shard_map.158 = (bf16[32,1024]{1,0:T(8,128)(2,1)}, f32[256,2]{1,0:T(8,128)}) custom-call(bf16[32,1024]{1,0:T(8,128)(2,1)} %tokens.1, s32[1,256]{1,0:T(1,128)} %bitcast.5, bf16[32,256]{1,0:T(8,128)(2,1)} %down_q.1, bf16[32,256]{1,0:T(8,128)(2,1)} %down_k.1, bf16[32,32]{1,0:T(8,128)(2,1)} %down_r.1, f32[1,256]{1,0:T(1,128)} %bitcast.6, f32[1,256]{1,0:T(1,128)} %bitcast.7, ...), custom_call_target="tpu_custom_call" | custom-call | tf_op jit(solution)/shard_map/pallas_call | solution.py:496
  151.3 1.6 %copy.18 = f32[256,2]{0,1:T(2,128)} copy(f32[256,2]{1,0:T(8,128)} %get-tuple-element.3) | data formatting | bytes 4096 | tf_op jit(solution)/shard_map/pallas_call | solution.py:496
  152.9 1.5 copy.20
where the time goes:
time: 155 us; the launch traced here: 154 us
  Pallas kernels  149 us (96%)
  local copies, waits for them, and re-layouts  4.45 us (3%)
    pallas_call x1, Pallas kernels, on_device(): pl.pallas_call(functools.partial(kernel, n, ntp, heads), out_shape=(jax.S...  149 us

commit v1 on v0

v1 whole, which is shorter than its diff:
```python
import functools
import math

import jax
import jax.numpy as jnp
import numpy as np
from jax import lax
from jax.experimental import pallas as pl
from jax.experimental.pallas import tpu as pltpu
from jax.sharding import PartitionSpec as P

NOPE = 64
ROPE = 32
VDIM = 64
THETA = 10000.0
EPS = 1e-06
MASKED = -1e30
MESH = pl.DeviceIdType.MESH
F32 = jnp.float32
BF16 = jnp.bfloat16
NX, NY, NZ = 4, 4, 8
NEAR = (0, 1, 7, 2, 6, 3, 5, 4)
ZPOS = {rel: pos for pos, rel in enumerate(NEAR)}


def dot(a, b):
    return jnp.dot(a, b, preferred_element_type=F32)


def dot_t(a, b):
    return lax.dot_general(a, b, (((1,), (1,)), ((), ())), preferred_element_type=F32)


def rms(values, gain):
    wide = values.astype(F32)
    scale = lax.rsqrt(jnp.mean(wide * wide, axis=-1, keepdims=True) + EPS)
    return (wide * scale * gain).astype(BF16)


def tables(n, block, heads):
    half = ROPE // 2
    inverse = np.float32(THETA) ** (-np.arange(half, dtype=np.float32) / np.float32(half))
    inverse = inverse.astype(np.float32).astype(np.float64)[None, :]

    def turn(positions):
        angles = positions.astype(np.float64)[:, None] * inverse
        both = np.zeros((len(positions), 256), np.float32)
        both[:, :ROPE] = np.tile(np.cos(angles), (1, 2))
        both[:, 128 : 128 + ROPE] = np.tile(np.sin(angles), (1, 2))
        return both

    width = NOPE + ROPE
    pick = np.zeros((heads * width, heads * 384), np.float32)
    eye = np.arange(NOPE)
    rot = np.arange(ROPE)
    low = np.arange(half)
    for head in range(heads):
        pick[head * width + eye, head * 384 + (head % 2) * NOPE + eye] = 1
        pick[head * width + NOPE + rot, head * 384 + 128 + rot] = 1
        pick[head * width + NOPE + half + low, head * 384 + 256 + low] = -1
        pick[head * width + NOPE + low, head * 384 + 256 + half + low] = 1
    pick_key = np.zeros((ROPE, 256), np.float32)
    pick_key[rot, rot] = 1
    pick_key[half + low, 128 + low] = -1
    pick_key[low, 128 + half + low] = 1
    return turn(np.arange(block)), turn(np.arange(n) * block), pick, pick_key


def kernel(
    n, ntp, heads,
    tokens, docs, down_q, down_k, down_r, gain_q, gain_k, up_q, up_k, up_v, out_wt, gain_o,
    turn_in, turn_block, pick, pick_key,
    out, log_out,
    tok, w, wr, uq, up, wo, uq_flat, up_flat, ql, kown, koth, ks, tab, kdoc, qdoc, sel, qs,
    sbuf, vbuf, top_s, sum_s, acc_s, att, prod, part, got_core, got_y, send_y,
    loc, s_tok, r_tok, s_w, r_w, s_wr, r_wr, s_uq, r_uq, s_up, r_up, s_wo, r_wo,
    s_q, r_q, s_a, r_a, s_z, r_z, s_b, r_b, s_d, r_d, s_f, r_f,
):
    me = lax.axis_index("sp")
    t = lax.axis_index("tp")
    z, x = me // NX, lax.rem(me, NX)
    y, core = t // 2, lax.rem(t, 2)
    own, width = tokens.shape
    block = ntp * own
    rows_all = heads * block

    def wrap(v, size):
        return lax.rem(v + size, size)

    def dev(dz=0, dx=0, dy=0, c=None):
        c = core if c is None else c
        zz = wrap(z + dz, NZ) if dz else z
        xx = wrap(x + dx, NX) if dx else x
        yy = wrap(y + dy, NY) if dy else y
        return (zz * NX + xx, yy * 2 + c)

    def dev_b(d):
        bx, by = dev(dx=d), dev(dy=d)
        return (jnp.where(core == 0, by[0], bx[0]), jnp.where(core == 0, by[1], bx[1]))

    c_dev = dev(c=1 - core)

    def rc(src, dst, s, r, device):
        return pltpu.make_async_remote_copy(
            src_ref=src, dst_ref=dst, send_sem=s, recv_sem=r, device_id=device, device_id_type=MESH
        )

    sends = []

    def send(make, which=None):
        make().start()
        sends.append((make, which))

    c_tok = pltpu.make_async_copy(tokens, tok.at[core], loc.at[0])
    c_tok.start()

    @pl.when(core == 0)
    def _():
        pltpu.make_async_copy(down_k, w.at[z, x], loc.at[1]).start()

    @pl.when(core == 1)
    def _():
        pltpu.make_async_copy(down_q, w.at[z, x], loc.at[1]).start()

    c_w = pltpu.make_async_copy(down_k, w.at[z, x], loc.at[1])
    c_wr = pltpu.make_async_copy(down_r, wr.at[z, x], loc.at[2])
    nq, nk = up_q.shape[1], up_k.shape[1]
    c_uq = pltpu.make_async_copy(up_q, uq.at[z, x], loc.at[3])
    c_up = [
        pltpu.make_async_copy(up_k, up.at[z, x, :, pl.ds(0, nk)], loc.at[4]),
        pltpu.make_async_copy(up_v, up.at[z, x, :, pl.ds(nk, nk)], loc.at[5]),
    ]
    c_wo = pltpu.make_async_copy(out_wt, wo.at[z, x], loc.at[6])
    c_tab = pltpu.make_async_copy(turn_in, tab, loc.at[7])
    c_sel = pltpu.make_async_copy(pick, sel, loc.at[8])
    for copy in [c_wr, c_uq] + c_up + [c_wo, c_tab, c_sel]:
        copy.start()

    barrier = pltpu.get_barrier_semaphore()
    others = [dev(dz=d) for d in range(1, NZ)] + [dev(dx=d) for d in range(1, NX)]
    others += [dev(dy=d) for d in range(1, NY)] + [dev(dy=d, c=1 - core) for d in range(NY)]
    for device in others:
        pl.semaphore_signal(barrier, inc=1, device_id=device, device_id_type=MESH)

    down = lax.broadcasted_iota(jnp.int32, (block, block), 0)
    across = lax.broadcasted_iota(jnp.int32, (block, block), 1)
    doc_row = jnp.broadcast_to(docs[...].astype(F32), (block, block))
    doc_col = jnp.sum(jnp.where(down == across, doc_row, 0.0), axis=-1, keepdims=True)
    lane = lax.broadcasted_iota(jnp.int32, (block, 128), 1)
    in_docs = (lane >= ROPE) & (lane < ROPE + n)
    same = doc_col == (lane - ROPE).astype(F32)
    kdoc[...] = jnp.where(in_docs & same, 1.0, 0.0)
    qdoc[...] = jnp.where(in_docs & jnp.logical_not(same), MASKED, 0.0)
    c_tab.wait()
    block_turn = turn_block[pl.ds(me, 1), :]
    cos_a, sin_a = block_turn[:, :128], block_turn[:, 128:]
    cos_b, sin_b = tab[:, :128], tab[:, 128:]
    tab[:, :128] = cos_a * cos_b - sin_a * sin_b
    tab[:, 128:] = sin_a * cos_b + cos_a * sin_b

    for copy in [c_w, c_wr, c_tok, c_uq] + c_up + [c_wo, c_sel]:
        copy.wait()
    pl.semaphore_wait(barrier, len(others))

    class Gather:
        def __init__(self, ref, s, r, which=None):
            self.ref, self.s, self.r, self.which = ref, s, r, which

        def start_z(self):
            for d in NEAR[1:]:
                send(lambda d=d: rc(self.ref.at[z, x], self.ref.at[z, x], self.s.at[d], self.r.at[d], dev(dz=d)), self.which)

        def start_x(self, d):
            for k in (1, 3, 2):
                def make(k=k):
                    ref = self.ref.at[wrap(z - d, NZ), x]
                    return rc(ref, ref, self.s.at[8 * k + d], self.r.at[8 * k + d], dev(dx=k))
                send(make, self.which)

        def from_z(self, d):
            ref = self.ref.at[wrap(z - d, NZ), x]
            rc(ref, ref, self.s.at[d], self.r.at[d], c_dev).wait_recv()

        def from_x(self, d, k):
            ref = self.ref.at[wrap(z - d, NZ), wrap(x - k, NX)]
            rc(ref, ref, self.s.at[8 * k + d], self.r.at[8 * k + d], c_dev).wait_recv()

        def start_all_x(self):
            for d in NEAR[1:]:
                self.from_z(d)
            for k in (1, 3, 2):
                def make(k=k):
                    ref = self.ref.at[:, x]
                    return rc(ref, ref, self.s.at[8 * k], self.r.at[8 * k], dev(dx=k))
                send(make, self.which)

        def from_all_x(self):
            for k in (1, 3, 2):
                ref = self.ref.at[:, wrap(x - k, NX)]
                rc(ref, ref, self.s.at[8 * k], self.r.at[8 * k], c_dev).wait_recv()

    g_w = Gather(w, s_w, r_w)
    g_wr = Gather(wr, s_wr, r_wr, 0)
    g_uq = Gather(uq, s_uq, r_uq)
    g_up = Gather(up, s_up, r_up)
    g_wo = Gather(wo, s_wo, r_wo)

    g_w.start_z()
    g_w.start_x(0)

    @pl.when(core == 0)
    def _():
        g_wr.start_z()
        g_wr.start_x(0)

    send(lambda: rc(tok.at[core], tok.at[core], s_tok.at[0], r_tok.at[0], c_dev))
    g_up.start_z()
    g_uq.start_z()
    for d in NEAR[1:]:
        g_w.from_z(d)
        g_w.start_x(d)

        @pl.when(core == 0)
        def _():
            g_wr.from_z(d)
            g_wr.start_x(d)

    g_up.start_all_x()
    g_uq.start_all_x()
    g_wo.start_z()

    rc(tok.at[1 - core], tok.at[1 - core], s_tok.at[0], r_tok.at[0], c_dev).wait_recv()
    gain = jnp.where(core == 0, gain_k[...], gain_q[...])
    for d in NEAR:
        for k in (1, 3, 2):
            g_w.from_x(d, k)

    chip_tokens = tok[...].reshape(2 * own, width)
    raw = dot(chip_tokens, w[...].reshape(width, w.shape[-1])).astype(BF16)
    lat = rms(raw, gain)

    @pl.when(core == 0)
    def _():
        for d in NEAR:
            for k in (1, 3, 2):
                g_wr.from_x(d, k)
        rotary = dot(chip_tokens, wr[...].reshape(width, ROPE)).astype(BF16)
        both = dot(rotary, pick_key[...])
        rows = pl.ds(pl.multiple_of(y * (2 * own), 2 * own), 2 * own)
        turned = both[:, :128] * tab[rows, :128] + both[:, 128:] * tab[rows, 128:] + kdoc[rows, :]
        for stripe in range(2):
            first = stripe * own
            half = own // 2
            parts = [
                lat[first + s * half : first + (s + 1) * half, h * 128 : (h + 1) * 128]
                for s in range(2)
                for h in range(2)
            ]
            packed = turned[first : first + half] + pltpu.roll(turned[first + half : first + own], 64, 1)
            parts.append(packed.astype(BF16))
            for i, tile in enumerate(parts):
                if stripe == 0:
                    kown[0, 0, 0, i] = tile
                else:
                    ks[i] = tile
        for k in (1, 3, 2):
            here = kown.at[0, 0, 0]
            there = kown.at[0, 0, (-k) % 4]
            send(lambda k=k: rc(kown.at[0, 0, 0], kown.at[0, 0, (-k) % 4], s_a.at[k], r_a.at[(-k) % 4], dev(dx=k)), 0)
            send(lambda k=k: rc(ks, kown.at[0, 0, (-k) % 4], s_a.at[4 + k], r_a.at[(-k) % 4], dev(dy=k, c=1)), 0)
        send(lambda: rc(ks, kown.at[0, 0, 0], s_a.at[4], r_a.at[0], dev(c=1)), 0)

    @pl.when(core == 1)
    def _():
        ql[y] = lat
        send(lambda: rc(ql.at[y], ql.at[y], s_q.at[0], r_q.at[0], dev(c=0)), 1)
        for k in (1, 3, 2):
            for c in range(2):
                send(lambda k=k, c=c: rc(ql.at[y], ql.at[y], s_q.at[4 * c + k], r_q.at[k], dev(dy=k, c=c)), 1)

    def z_recv(pos):
        if pos == 7:
            for half in range(2):
                ref = kown.at[0, 7, pl.ds(2 * half, 2)]
                rc(ref, ref, s_z.at[0], r_z.at[7 + half], c_dev).wait_recv()
        else:
            ref = kown.at[0, pos]
            rc(ref, ref, s_z.at[0], r_z.at[pos], c_dev).wait_recv()

    def z_send(slot, src_pos, d, total, pieces=None):
        pos = ZPOS[(-total) % NZ]
        if pieces is None:
            send(lambda: rc(kown.at[0, src_pos], kown.at[0, pos], s_z.at[slot], r_z.at[pos], dev(dz=d)))
        else:
            part_of = pl.ds(2 * pieces, 2)
            send(lambda: rc(kown.at[0, src_pos, part_of], kown.at[0, 7, part_of], s_z.at[slot], r_z.at[7 + pieces], dev(dz=d)))

    def b_send(pos):
        send(lambda: rc(kown.at[0, pos], kown.at[3, pos], s_b.at[pos], r_b.at[24 + pos], dev_b(1)))
        send(lambda: rc(kown.at[0, pos], kown.at[1, pos], s_b.at[8 + pos], r_b.at[8 + pos], dev_b(-1)))

    def d_send(b, pos):
        send(lambda: rc(kown.at[b, pos], koth.at[b, pos], s_d.at[8 * b + pos], r_d.at[8 * b + pos], c_dev))

    def d_recv(b, pos):
        ref = koth.at[b, pos]
        rc(ref, ref, s_d.at[8 * b + pos], r_d.at[8 * b + pos], c_dev).wait_recv()

    def first_row():
        @pl.when(core == 1)
        def _():
            ref = kown.at[0, 0, 0]
            rc(ref, ref, s_a.at[0], r_a.at[0], c_dev).wait_recv()

        for k in (1, 3, 2):
            ref = kown.at[0, 0, k]
            rc(ref, ref, s_a.at[0], r_a.at[k], c_dev).wait_recv()
        z_send(0, 0, 2, 2)
        z_send(1, 0, -2, -2)
        z_send(2, 0, 1, 1)
        z_send(3, 0, -1, -1)
        b_send(0)
        d_send(0, 0)

    def z_row(pos):
        z_recv(pos)
        if NEAR[pos] == 6:
            z_send(4, pos, 1, 3)
            z_send(5, pos, 2, 4, 0)
        if NEAR[pos] == 2:
            z_send(6, pos, -1, -3)
            z_send(7, pos, -2, -4, 1)
        b_send(pos)
        d_send(0, pos)

    def b_row(b, pos):
        ref = kown.at[b, pos]
        rc(ref, ref, s_b.at[0], r_b.at[8 * b + pos], c_dev).wait_recv()
        half = 0 if b == 3 else 1
        part_of = pl.ds(2 * half, 2)
        send(
            lambda: rc(
                kown.at[b, pos, part_of], kown.at[2, pos, part_of],
                s_b.at[16 + 8 * half + pos], r_b.at[16 * half + pos], dev_b(1 if b == 3 else -1),
            )
        )
        d_send(b, pos)

    def far_row(pos):
        for half in range(2):
            ref = kown.at[2, pos, pl.ds(2 * half, 2)]
            rc(ref, ref, s_b.at[0], r_b.at[16 * half + pos], c_dev).wait_recv()
        d_send(2, pos)

    first_row()
    g_up.from_all_x()
    g_uq.from_all_x()
    for j in range(n):
        up_flat[j * 8 : (j + 1) * 8, :] = up[j // NX, j % NX]
        uq_flat[j * 8 : (j + 1) * 8, :] = uq[j // NX, j % NX]
    for k in range(NY):
        def wait_q(k=k):
            ref = ql.at[wrap(y - k, NY)]
            rc(ref, ref, s_q.at[0], r_q.at[k], c_dev).wait_recv()
        if k == 0:
            pl.when(core == 0)(wait_q)
        else:
            wait_q()

    scale = 1.0 / math.sqrt(NOPE + ROPE)
    factor = scale * math.log2(math.e)
    projected = dot(ql[...].reshape(block, ql.shape[-1]), uq_flat[...]).astype(BF16)
    for head in range(heads):
        laid = dot(projected, sel[:, head * 384 : (head + 1) * 384])
        turned = (laid[:, 128:256] * tab[:, :128] + laid[:, 256:] * tab[:, 128:]) * factor + qdoc[...]
        plain = (laid[:, :128] * factor).astype(BF16)
        rows = pl.ds(head * block, block)
        qs[0, rows, :128] = plain
        qs[1, rows, :128] = plain
        qs[0, rows, 128:] = turned.astype(BF16)
        qs[1, rows, 128:] = pltpu.roll(turned, 64, 1).astype(BF16)

    def score(ref, b, h, par):
        for s in range(2):
            def tiles(i):
                return ref[b, 4 * h : 4 * h + 4, :, i].reshape(256, 128)

            kv = dot(jnp.concatenate([tiles(2 * s), tiles(2 * s + 1)], axis=1), up_flat[...]).astype(BF16)
            keys = jnp.concatenate([kv[:, :nk], tiles(4)], axis=1)
            vbuf[par, s * 256 : (s + 1) * 256, :] = kv[:, nk:]
            sbuf[par, s] = dot_t(qs[s], keys)

    step = 128

    def weigh(par, first):
        for r in range(0, rows_all, step):
            rows = pl.ds(r, step)
            parts = [sbuf[par, s, rows, h * 128 : (h + 1) * 128] for s in range(2) for h in range(2)]
            most = jnp.maximum(jnp.maximum(parts[0], parts[1]), jnp.maximum(parts[2], parts[3]))
            most = jnp.max(most, axis=-1, keepdims=True)
            if first:
                new = jnp.broadcast_to(most, (step, 128))
            else:
                old = top_s[rows, :]
                new = jnp.maximum(old, most)
                alpha = jnp.exp2(old - new)
            weights = [jnp.exp2(p - new) for p in parts]
            total = (weights[0] + weights[1]) + (weights[2] + weights[3])
            mixed = dot(jnp.concatenate([p.astype(BF16) for p in weights], axis=1), vbuf[par])
            top_s[rows, :] = new
            if first:
                sum_s[rows, :] = total
                acc_s[rows, :] = mixed
            else:
                sum_s[rows, :] = sum_s[rows, :] * alpha + total
                acc_s[rows, :] = acc_s[rows, :] * alpha + mixed

    groups = []
    for b, h in ((0, 0), (0, 1), (1, 0), (3, 0), (1, 1), (3, 1), (2, 0), (2, 1)):
        groups.append((kown, b, h))
        groups.append((koth, b, h))
    events = {
        0: [lambda p=p: z_row(p) for p in (1, 2, 3, 4)],
        1: [lambda: b_row(1, 0), lambda: b_row(3, 0), lambda: z_row(5), lambda: z_row(6)],
        2: [lambda: z_row(7), lambda: b_row(1, 1), lambda: b_row(3, 1)],
        3: [lambda: b_row(1, 2), lambda: b_row(3, 2), g_wo.start_all_x],
        4: [lambda: b_row(1, 3), lambda: b_row(3, 3)],
        5: [lambda: b_row(1, 4), lambda: b_row(3, 4), lambda: far_row(0)],
        6: [lambda: b_row(1, 5), lambda: b_row(3, 5), lambda: far_row(1)],
        7: [lambda: b_row(1, 6), lambda: b_row(3, 6), lambda: far_row(2)],
        8: [lambda: b_row(1, 7), lambda: b_row(3, 7), lambda: far_row(3)],
        9: [lambda: far_row(4)],
        10: [lambda: far_row(5)],
        11: [lambda: far_row(6), lambda: far_row(7)],
    }
    for j, (ref, b, h) in enumerate(groups):
        for event in events.get(j, ()):
            event()
        if ref is koth:
            for pos in range(4 * h, 4 * h + 4):
                d_recv(b, pos)
        score(ref, b, h, j % 2)
        if j > 0:
            weigh((j - 1) % 2, j == 1)
    weigh((len(groups) - 1) % 2, False)

    head_lane = lax.broadcasted_iota(jnp.int32, (block, nk), 1) // VDIM
    attended = jnp.zeros((block, nk), F32)
    sums = []
    for head in range(heads):
        rows = pl.ds(head * block, block)
        weight_sum = jnp.sum(sum_s[rows, :], axis=-1, keepdims=True)
        attended = jnp.where(head_lane == head, acc_s[rows, :] / weight_sum, attended)
        sums.append(top_s[rows, :1] * math.log(2.0) + jnp.log(weight_sum))
    log_out[...] = jnp.concatenate(sums, axis=1)
    att[...] = attended.astype(BF16)

    g_wo.from_all_x()
    whole = dot_t(att[...], wo[...].reshape(width, nk))
    prod[...] = whole.reshape(NY, 2, own, width)

    def f_c(k):
        return rc(part.at[k], got_core.at[k], s_f.at[k], r_f.at[k], c_dev)

    def f_y(k):
        return rc(send_y.at[k], got_y.at[k], s_f.at[NY + k], r_f.at[NY + k], dev(dy=k))

    order = (2, 1, 3, 0)
    for k in order:
        part[k] = prod[wrap(y + k, NY), 1 - core].astype(BF16)
        send(lambda k=k: f_c(k))
    for k in order[:-1]:
        far = prod[wrap(y + k, NY), core]
        f_c(k).wait_recv()
        send_y[k] = (far + got_core[k].astype(F32)).astype(BF16)
        send(lambda k=k: f_y(k))
    near = prod[y, core]
    f_c(0).wait_recv()
    near = near + got_core[0].astype(F32)
    for k in order[:-1]:
        f_y(k).wait_recv()
        near = near + got_y[k].astype(F32)
    out[...] = rms(near.astype(BF16), gain_o[...])

    for make, which in sends:
        if which is None:
            make().wait_send()
    for c in range(2):
        @pl.when(core == c)
        def _():
            for make, which in sends:
                if which == c:
                    make().wait_send()


def on_device(n, ntp, tokens, doc_ids, down_q, down_k, down_r, gain_q, gain_k, up_q, up_k, up_v, out_w, gain_o):
    own, width = tokens.shape
    block = doc_ids.shape[0]
    heads = up_k.shape[1] // NOPE
    rank = down_k.shape[1]
    nq, nk, nv = up_q.shape[1], up_k.shape[1], up_v.shape[1]
    turn_in, turn_block, pick, pick_key = tables(n, block, heads)
    vmem = pl.BlockSpec(memory_space=pltpu.VMEM)
    hbm = pl.BlockSpec(memory_space=pl.ANY)
    dma = lambda k: pltpu.SemaphoreType.DMA((k,))
    v = lambda *shape, dtype=BF16: pltpu.VMEM(shape, dtype)
    rows = heads * block
    scratch = [
        v(2, own, width), v(NZ, NX, width // n, rank), v(NZ, NX, width // n, ROPE),
        v(NZ, NX, rank // n, nq), v(NZ, NX, rank // n, nk + nv), v(NZ, NX, width // n, nv),
        v(rank, nq), v(rank, nk + nv), v(NY, 2 * own, rank),
        v(4, NZ, 4, 5, own // 2, 128), v(4, NZ, 4, 5, own // 2, 128), v(5, own // 2, 128),
        v(block, 256, dtype=F32), v(block, 128, dtype=F32), v(block, 128, dtype=F32), v(*pick.shape),
        v(2, rows, 256),
        v(2, 2, rows, 256, dtype=F32), v(2, 512, nv),
        v(rows, 128, dtype=F32), v(rows, 128, dtype=F32), v(rows, 128, dtype=F32),
        v(block, nv), v(NY, 2, own, width, dtype=F32),
        v(NY, own, width), v(NY, own, width), v(NY, own, width), v(NY, own, width),
        dma(9), dma(1), dma(1), dma(32), dma(32), dma(32), dma(32), dma(32), dma(32), dma(32), dma(32), dma(32), dma(32),
        dma(8), dma(4), dma(8), dma(4), dma(8), dma(9), dma(32), dma(32), dma(32), dma(32), dma(8), dma(8),
    ]
    return pl.pallas_call(
        functools.partial(kernel, n, ntp, heads),
        out_shape=(
            jax.ShapeDtypeStruct((own, width), BF16),
            jax.ShapeDtypeStruct((block, heads), F32),
        ),
        in_specs=[hbm, vmem, hbm, hbm, hbm, vmem, vmem, hbm, hbm, hbm, hbm, vmem, hbm, vmem, hbm, vmem],
        out_specs=(vmem, vmem),
        scratch_shapes=scratch,
        compiler_params=pltpu.CompilerParams(
            collective_id=0, has_side_effects=True, vmem_limit_bytes=60 * 1024 * 1024
        ),
    )(
        tokens, doc_ids[None, :], down_q, down_k, down_r, gain_q[None, :], gain_k[None, :],
        up_q, up_k, up_v, out_w.T, gain_o[None, :],
        jnp.asarray(turn_in), jnp.asarray(turn_block), jnp.asarray(pick, BF16), jnp.asarray(pick_key, BF16),
    )


def solution(mesh):
    assert mesh.shape["tp"] == 2 * NY and mesh.shape["sp"] == NX * NZ
    placed = (
        P(("sp", "tp"), None), P("sp"), P("sp", None), P("sp", None), P("sp", None), P(), P(),
        P("sp", "tp"), P("sp", "tp"), P("sp", "tp"), P("tp", "sp"), P(),
    )
    return jax.shard_map(
        functools.partial(on_device, mesh.shape["sp"], mesh.shape["tp"]),
        mesh=mesh,
        in_specs=placed,
        out_specs=(P(("sp", "tp"), None), P("sp", "tp")),
        check_vma=False,
    )
```

time: 155 us -> 69.9 us (0.45)
  Pallas kernels: 149 us -> 66.9 us
  local copies, waits for them, and re-layouts: 4.45 us -> 2.23 us
    pallas_call x1, Pallas kernels: 149 us -> 66.9 us  [on_device(): pl.pallas_call(functools.partial(kernel, n, ntp, heads), out_shape=(jax.S...]
    unnamed x2 -> x3, local copies, waits for them, and re-layouts: 2.89 us -> 0.63 us
where the time goes in v1:
time: 69.9 us; the launch traced here: 69.7 us
  Pallas kernels  66.9 us (96%)
  local copies, waits for them, and re-layouts  2.23 us (3%)
    pallas_call x1, Pallas kernels, on_device(): pl.pallas_call(functools.partial(kernel, n, ntp, heads), out_shape=(jax.S...  66.9 us
    pallas_call x1, local copies, waits for them, and re-layouts, on_device(): pl.pallas_call(functools.partial(kernel, n, ntp, heads), out_shape=(jax.S...  1.59 us

profile of v1, /device:TPU:1, one launch (start us, length us, event | category | flops | bytes accessed | tf_op | source)
XLA Modules:
  0.0 69.7 jit_solution(104133172404093280)
XLA Ops:
  0.6 66.9 %shard_map.167 = (bf16[32,1024]{1,0:T(8,128)(2,1)}, f32[256,2]{1,0:T(8,128)}) custom-call(bf16[32,1024]{1,0:T(8,128)(2,1)} %tokens.1, s32[1,256]{1,0:T(1,128)} %bitcast.7, bf16[32,256]{1,0:T(8,128)(2,1)} %down_q.1, bf16[32,256]{1,0:T(8,128)(2,1)} %down_k.1, bf16[32,32]{1,0:T(8,128)(2,1)} %down_r.1, f32[1,256]{1,0:T(1,128)} %bitcast.8, f32[1,256]{1,0:T(1,128)} %bitcast.9, ...), custom_call_target="tpu_custom_call" | custom-call | tf_op jit(solution)/shard_map/pallas_call | solution.py:522
  67.5 0.0 copy-start
  67.5 1.6 %copy.18 = f32[256,2]{0,1:T(2,128)} copy(f32[256,2]{1,0:T(8,128)} %get-tuple-element.3) | data formatting | bytes 4096 | tf_op jit(solution)/shard_map/pallas_call | solution.py:522
  69.1 0.0 copy-done
  69.1 0.6 copy.20
Async XLA Ops:
  67.5 1.6 %copy-start = (bf16[32,1024]{1,0:T(8,128)(2,1)S(1)}, bf16[32,1024]{1,0:T(8,128)(2,1)}, u32[]{:S(2)}) copy-start(bf16[32,1024]{1,0:T(8,128)(2,1)} %get-tuple-element.6) | copy-start | bytes 196612

commit v2 on v1

v2 whole, which is shorter than its diff:
```python
import functools
import math

import jax
import jax.numpy as jnp
import numpy as np
from jax import lax
from jax.experimental import pallas as pl
from jax.experimental.pallas import tpu as pltpu
from jax.sharding import PartitionSpec as P

NOPE = 64
ROPE = 32
VDIM = 64
THETA = 10000.0
EPS = 1e-06
MASKED = -1e30
MESH = pl.DeviceIdType.MESH
F32 = jnp.float32
BF16 = jnp.bfloat16
NX, NY, NZ = 4, 4, 8
NEAR = (0, 1, 7, 2, 6, 3, 5, 4)
ZPOS = {rel: pos for pos, rel in enumerate(NEAR)}


def dot(a, b):
    return jnp.dot(a, b, preferred_element_type=F32)


def dot_t(a, b):
    return lax.dot_general(a, b, (((1,), (1,)), ((), ())), preferred_element_type=F32)


def rms(values, gain):
    wide = values.astype(F32)
    scale = lax.rsqrt(jnp.mean(wide * wide, axis=-1, keepdims=True) + EPS)
    return (wide * scale * gain).astype(BF16)


def tables(n, block, heads):
    half = ROPE // 2
    inverse = np.float32(THETA) ** (-np.arange(half, dtype=np.float32) / np.float32(half))
    inverse = inverse.astype(np.float32).astype(np.float64)[None, :]

    def turn(positions):
        angles = positions.astype(np.float64)[:, None] * inverse
        both = np.zeros((len(positions), 256), np.float32)
        both[:, :ROPE] = np.tile(np.cos(angles), (1, 2))
        both[:, 128 : 128 + ROPE] = np.tile(np.sin(angles), (1, 2))
        return both

    width = NOPE + ROPE
    pick = np.zeros((heads * width, heads * 384), np.float32)
    eye = np.arange(NOPE)
    rot = np.arange(ROPE)
    low = np.arange(half)
    for head in range(heads):
        pick[head * width + eye, head * 384 + (head % 2) * NOPE + eye] = 1
        pick[head * width + NOPE + rot, head * 384 + 128 + rot] = 1
        pick[head * width + NOPE + half + low, head * 384 + 256 + low] = -1
        pick[head * width + NOPE + low, head * 384 + 256 + half + low] = 1
    pick_key = np.zeros((ROPE, 256), np.float32)
    pick_key[rot, rot] = 1
    pick_key[half + low, 128 + low] = -1
    pick_key[low, 128 + half + low] = 1
    return turn(np.arange(block)), turn(np.arange(n) * block), pick, pick_key


def kernel(
    n, ntp, heads,
    tokens, docs_in, down_q, down_k, down_r, gain_q, gain_k, up_q, up_k, up_v, out_wt, gain_o,
    turn_in, turn_block, pick, pick_key,
    out, log_out,
    docs, gain, gain_out, turn_me, sel_key,
    tok, w, wr, uq, up, wo, uq_flat, up_flat, ql, kown, koth, ks, tab, kdoc, qdoc, sel, qs,
    sbuf, vbuf, top_s, sum_s, acc_s, att, prod, part, got_core, got_y, send_y,
    loc, s_tok, r_tok, s_w, r_w, s_wr, r_wr, s_uq, r_uq, s_up, r_up, s_wo, r_wo,
    s_q, r_q, s_a, r_a, s_z, r_z, s_b, r_b, s_d, r_d, s_f, r_f,
):
    me = lax.axis_index("sp")
    t = lax.axis_index("tp")
    z, x = me // NX, lax.rem(me, NX)
    y, core = t // 2, lax.rem(t, 2)
    own, width = tokens.shape
    block = ntp * own
    rows_all = heads * block

    def wrap(v, size):
        return lax.rem(v + size, size)

    def dev(dz=0, dx=0, dy=0, c=None):
        c = core if c is None else c
        zz = wrap(z + dz, NZ) if dz else z
        xx = wrap(x + dx, NX) if dx else x
        yy = wrap(y + dy, NY) if dy else y
        return (zz * NX + xx, yy * 2 + c)

    def dev_b(d):
        bx, by = dev(dx=d), dev(dy=d)
        return (jnp.where(core == 0, by[0], bx[0]), jnp.where(core == 0, by[1], bx[1]))

    c_dev = dev(c=1 - core)

    def rc(src, dst, s, r, device):
        return pltpu.make_async_remote_copy(
            src_ref=src, dst_ref=dst, send_sem=s, recv_sem=r, device_id=device, device_id_type=MESH
        )

    def sent(ref, s):
        rc(ref, ref, s, s, c_dev).wait_send()

    def got(ref, r):
        rc(ref, ref, r, r, c_dev).wait_recv()

    barrier = pltpu.get_barrier_semaphore()
    others = [dev(dz=d) for d in range(1, NZ)] + [dev(dx=d) for d in range(1, NX)]
    others += [dev(dy=d) for d in range(1, NY)] + [dev(dy=d, c=1 - core) for d in range(NY)]
    for device in others:
        pl.semaphore_signal(barrier, inc=1, device_id=device, device_id_type=MESH)

    @pl.when(core == 0)
    def _():
        pltpu.make_async_copy(down_k, w.at[z, x], loc.at[1]).start()
        pltpu.make_async_copy(gain_k, gain, loc.at[9]).start()

    @pl.when(core == 1)
    def _():
        pltpu.make_async_copy(down_q, w.at[z, x], loc.at[1]).start()
        pltpu.make_async_copy(gain_q, gain, loc.at[9]).start()

    nq, nk = up_q.shape[1], up_k.shape[1]
    c_w = pltpu.make_async_copy(down_k, w.at[z, x], loc.at[1])
    c_gain = pltpu.make_async_copy(gain_k, gain, loc.at[9])
    c_docs = pltpu.make_async_copy(docs_in, docs, loc.at[10])
    c_tab = pltpu.make_async_copy(turn_in, tab, loc.at[7])
    c_me = pltpu.make_async_copy(turn_block.at[me], turn_me, loc.at[11])
    c_tok = pltpu.make_async_copy(tokens, tok.at[core], loc.at[0])
    c_wr = pltpu.make_async_copy(down_r, wr.at[z, x], loc.at[2])
    c_uq = pltpu.make_async_copy(up_q, uq.at[z, x], loc.at[3])
    c_up = [
        pltpu.make_async_copy(up_k, up.at[z, x, :, pl.ds(0, nk)], loc.at[4]),
        pltpu.make_async_copy(up_v, up.at[z, x, :, pl.ds(nk, nk)], loc.at[5]),
    ]
    c_wo = pltpu.make_async_copy(out_wt, wo.at[z, x], loc.at[6])
    c_sel = pltpu.make_async_copy(pick, sel, loc.at[8])
    c_key = pltpu.make_async_copy(pick_key, sel_key, loc.at[12])
    c_out = pltpu.make_async_copy(gain_o, gain_out, loc.at[13])
    for copy in [c_docs, c_tab, c_me, c_wr, c_tok, c_uq] + c_up + [c_key, c_wo, c_sel, c_out]:
        copy.start()

    down = lax.broadcasted_iota(jnp.int32, (block, block), 0)
    across = lax.broadcasted_iota(jnp.int32, (block, block), 1)
    c_docs.wait()
    doc_row = jnp.broadcast_to(docs[...].astype(F32), (block, block))
    doc_col = jnp.sum(jnp.where(down == across, doc_row, 0.0), axis=-1, keepdims=True)
    lane = lax.broadcasted_iota(jnp.int32, (block, 128), 1)
    in_docs = (lane >= ROPE) & (lane < ROPE + n)
    same = doc_col == (lane - ROPE).astype(F32)
    kdoc[...] = jnp.where(in_docs & same, 1.0, 0.0)
    qdoc[...] = jnp.where(in_docs & jnp.logical_not(same), MASKED, 0.0)
    c_tab.wait()
    c_me.wait()
    cos_a, sin_a = turn_me[:, :128], turn_me[:, 128:]
    cos_b, sin_b = tab[:, :128], tab[:, 128:]
    tab[:, :128] = cos_a * cos_b - sin_a * sin_b
    tab[:, 128:] = sin_a * cos_b + cos_a * sin_b

    for copy in [c_w, c_wr, c_tok, c_uq] + c_up + [c_key, c_gain]:
        copy.wait()
    pl.semaphore_wait(barrier, len(others))

    class Batch:
        def __init__(self, ref, s, r):
            self.ref, self.s, self.r = ref, s, r

        def start_z(self):
            here = self.ref.at[z, x]
            for d in NEAR[1:]:
                rc(here, here, self.s.at[0], self.r.at[0], dev(dz=d)).start()

        def start_x(self):
            got(self.ref.at[pl.ds(0, NZ - 1), x], self.r.at[0])
            column = self.ref.at[:, x]
            rc(column, column, self.s.at[1], self.r.at[1], dev(dx=1)).start()
            rc(column, column, self.s.at[1], self.r.at[2], dev(dx=-1)).start()

        def start_far(self):
            got(self.ref.at[:, wrap(x - 1, NX)], self.r.at[1])
            low = self.ref.at[pl.ds(0, NZ // 2), wrap(x - 1, NX)]
            rc(low, low, self.s.at[1], self.r.at[3], dev(dx=1)).start()
            got(self.ref.at[:, wrap(x + 1, NX)], self.r.at[2])
            high = self.ref.at[pl.ds(NZ // 2, NZ // 2), wrap(x + 1, NX)]
            rc(high, high, self.s.at[1], self.r.at[3], dev(dx=-1)).start()

        def finish(self):
            got(self.ref.at[:, wrap(x + 2, NX)], self.r.at[3])

        def drain(self):
            sent(self.ref.at[pl.ds(0, NZ - 1), x], self.s.at[0])
            sent(self.ref.at[pl.ds(0, NZ - 2)], self.s.at[1])

    class Pieces(Batch):
        def start_z(self):
            here = self.ref.at[z, x]
            for d in NEAR[1:]:
                rc(here, here, self.s.at[0], self.r.at[d], dev(dz=d)).start()

        def x_of(self, d):
            here = self.ref.at[wrap(z - d, NZ), x]
            if d > 0:
                got(here, self.r.at[d])
            rc(here, here, self.s.at[1], self.r.at[8 + d], dev(dx=1)).start()
            rc(here, here, self.s.at[1], self.r.at[16 + d], dev(dx=-1)).start()

        def far_of(self, d):
            low = self.ref.at[wrap(z - d, NZ), wrap(x - 1, NX)]
            high = self.ref.at[wrap(z - d, NZ), wrap(x + 1, NX)]
            got(low, self.r.at[8 + d])
            if d in (0, 7, 6, 5):
                rc(low, low, self.s.at[1], self.r.at[0], dev(dx=1)).start()
            got(high, self.r.at[16 + d])
            if d in (1, 2, 3, 4):
                rc(high, high, self.s.at[1], self.r.at[0], dev(dx=-1)).start()

        def finish(self):
            got(self.ref.at[:, wrap(x + 2, NX)], self.r.at[0])

    g_k = Pieces(w, s_w, r_w)
    g_q = Batch(w, s_w, r_w)
    g_wr = Batch(wr, s_wr, r_wr)
    g_uq = Batch(uq, s_uq, r_uq)
    g_up = Batch(up, s_up, r_up)
    g_wo = Batch(wo, s_wo, r_wo)
    here = tok.at[core]
    c_partner = rc(here, here, s_tok.at[0], r_tok.at[0], c_dev)

    @pl.when(core == 0)
    def _():
        g_k.start_z()
        g_k.x_of(0)
        g_wr.start_z()
        c_partner.start()
        g_up.start_z()
        g_uq.start_z()
        for d in (1, 7, 2, 6):
            g_k.x_of(d)
        g_k.far_of(0)
        for d in (3, 5):
            g_k.x_of(d)
        g_k.far_of(1)
        g_k.far_of(7)
        g_k.x_of(4)
        g_wr.start_x()
        for d in (2, 6, 3, 5, 4):
            g_k.far_of(d)
        g_wr.start_far()

    @pl.when(core == 1)
    def _():
        g_q.start_z()
        c_partner.start()
        g_up.start_z()
        g_uq.start_z()
        g_q.start_x()
        g_q.start_far()

    g_up.start_x()
    g_uq.start_x()
    got(tok.at[1 - core], r_tok.at[0])

    @pl.when(core == 0)
    def _():
        g_k.finish()
        g_wr.finish()

    @pl.when(core == 1)
    def _():
        g_q.finish()

    chip_tokens = tok[...].reshape(2 * own, width)
    raw = dot(chip_tokens, w[...].reshape(width, w.shape[-1])).astype(BF16)
    lat = rms(raw, gain[...])

    @pl.when(core == 0)
    def _():
        rotary = dot(chip_tokens, wr[...].reshape(width, ROPE)).astype(BF16)
        both = dot(rotary, sel_key[...])
        rows = pl.ds(pl.multiple_of(y * (2 * own), 2 * own), 2 * own)
        turned = both[:, :128] * tab[rows, :128] + both[:, 128:] * tab[rows, 128:] + kdoc[rows, :]
        for stripe in range(2):
            first = stripe * own
            half = own // 2
            parts = [
                lat[first + s * half : first + (s + 1) * half, h * 128 : (h + 1) * 128]
                for s in range(2)
                for h in range(2)
            ]
            packed = turned[first : first + half] + pltpu.roll(turned[first + half : first + own], 64, 1)
            parts.append(packed.astype(BF16))
            for i, tile in enumerate(parts):
                if stripe == 0:
                    kown[0, 0, 0, i] = tile
                else:
                    ks[i] = tile
        here = kown.at[0, 0, 0]
        rc(ks, here, s_a.at[1], r_a.at[0], dev(c=1)).start()
        for k in (2, 1, 3):
            there = kown.at[0, 0, (-k) % 4]
            rc(here, there, s_a.at[0], r_a.at[0], dev(dx=k)).start()
            rc(ks, there, s_a.at[1], r_a.at[0], dev(dy=k, c=1)).start()

    @pl.when(core == 1)
    def _():
        ql[y] = lat
        here = ql.at[y]
        for k in (2, 1, 3):
            for c in range(2):
                rc(here, here, s_q.at[c], r_q.at[0], dev(dy=k, c=c)).start()
        rc(here, here, s_q.at[0], r_q.at[0], dev(c=0)).start()

    def z_send(src_pos, d, total, pieces=None):
        pos = ZPOS[(-total) % NZ]
        part_of = pl.ds(0, 4) if pieces is None else pl.ds(2 * pieces, 2)
        rc(kown.at[0, src_pos, part_of], kown.at[0, pos, part_of], s_z.at[0], r_z.at[pos], dev(dz=d)).start()

    def b_send(pos):
        rc(kown.at[0, pos], kown.at[3, pos], s_b.at[0], r_b.at[24 + pos], dev_b(1)).start()
        rc(kown.at[0, pos], kown.at[1, pos], s_b.at[0], r_b.at[8 + pos], dev_b(-1)).start()

    def d_send(b, pos):
        rc(kown.at[b, pos], koth.at[b, pos], s_d.at[0], r_d.at[2 * b + pos // 4], c_dev).start()

    def first_row():
        @pl.when(core == 0)
        def _():
            got(kown.at[0, 0, pl.ds(1, 3)], r_a.at[0])

        @pl.when(core == 1)
        def _():
            got(kown.at[0, 0], r_a.at[0])

        z_send(0, 2, 2)
        z_send(0, -2, -2)
        z_send(0, 1, 1)
        z_send(0, -1, -1)
        b_send(0)
        d_send(0, 0)

    def z_row(pos):
        got(kown.at[0, pos], r_z.at[pos])
        if NEAR[pos] == 6:
            z_send(pos, 1, 3)
            z_send(pos, 2, 4, 0)
        if NEAR[pos] == 2:
            z_send(pos, -1, -3)
            z_send(pos, -2, -4, 1)
        b_send(pos)
        d_send(0, pos)

    def b_row(b, pos):
        got(kown.at[b, pos], r_b.at[8 * b + pos])
        half = 0 if b == 3 else 1
        part_of = pl.ds(2 * half, 2)
        rc(
            kown.at[b, pos, part_of], kown.at[2, pos, part_of], s_b.at[0], r_b.at[pos], dev_b(1 if b == 3 else -1)
        ).start()
        d_send(b, pos)

    def far_row(pos):
        got(kown.at[2, pos], r_b.at[pos])
        d_send(2, pos)

    first_row()
    g_up.start_far()
    g_uq.start_far()
    g_up.finish()
    g_uq.finish()
    for j in range(n):
        up_flat[j * 8 : (j + 1) * 8, :] = up[j // NX, j % NX]
        uq_flat[j * 8 : (j + 1) * 8, :] = uq[j // NX, j % NX]

    @pl.when(core == 0)
    def _():
        got(ql, r_q.at[0])

    @pl.when(core == 1)
    def _():
        got(ql.at[pl.ds(0, 3)], r_q.at[0])

    c_sel.wait()
    scale = 1.0 / math.sqrt(NOPE + ROPE)
    factor = scale * math.log2(math.e)
    projected = dot(ql[...].reshape(block, ql.shape[-1]), uq_flat[...]).astype(BF16)
    for head in range(heads):
        laid = dot(projected, sel[:, head * 384 : (head + 1) * 384])
        turned = (laid[:, 128:256] * tab[:, :128] + laid[:, 256:] * tab[:, 128:]) * factor + qdoc[...]
        plain = (laid[:, :128] * factor).astype(BF16)
        rows = pl.ds(head * block, block)
        qs[0, rows, :128] = plain
        qs[1, rows, :128] = plain
        qs[0, rows, 128:] = turned.astype(BF16)
        qs[1, rows, 128:] = pltpu.roll(turned, 64, 1).astype(BF16)

    def score(ref, b, h, par):
        for s in range(2):
            def tiles(i):
                return ref[b, 4 * h : 4 * h + 4, :, i].reshape(256, 128)

            kv = dot(jnp.concatenate([tiles(2 * s), tiles(2 * s + 1)], axis=1), up_flat[...]).astype(BF16)
            keys = jnp.concatenate([kv[:, :nk], tiles(4)], axis=1)
            vbuf[par, s * 256 : (s + 1) * 256, :] = kv[:, nk:]
            sbuf[par, s] = dot_t(qs[s], keys)

    step = 128

    def weigh(par, first):
        for r in range(0, rows_all, step):
            rows = pl.ds(r, step)
            parts = [sbuf[par, s, rows, h * 128 : (h + 1) * 128] for s in range(2) for h in range(2)]
            most = jnp.maximum(jnp.maximum(parts[0], parts[1]), jnp.maximum(parts[2], parts[3]))
            most = jnp.max(most, axis=-1, keepdims=True)
            if first:
                new = jnp.broadcast_to(most, (step, 128))
            else:
                old = top_s[rows, :]
                new = jnp.maximum(old, most)
                alpha = jnp.exp2(old - new)
            weights = [jnp.exp2(p - new) for p in parts]
            total = (weights[0] + weights[1]) + (weights[2] + weights[3])
            mixed = dot(jnp.concatenate([p.astype(BF16) for p in weights], axis=1), vbuf[par])
            top_s[rows, :] = new
            if first:
                sum_s[rows, :] = total
                acc_s[rows, :] = mixed
            else:
                sum_s[rows, :] = sum_s[rows, :] * alpha + total
                acc_s[rows, :] = acc_s[rows, :] * alpha + mixed

    groups = []
    for b, h in ((0, 0), (0, 1), (1, 0), (3, 0), (1, 1), (3, 1), (2, 0), (2, 1)):
        groups.append((kown, b, h))
        groups.append((koth, b, h))
    events = {
        0: [lambda p=p: z_row(p) for p in (1, 2, 3, 4)],
        1: [lambda: b_row(1, 0), lambda: b_row(3, 0), lambda: z_row(5), lambda: z_row(6)],
        2: [lambda: z_row(7), lambda: b_row(1, 1), lambda: b_row(3, 1)],
        3: [lambda: b_row(1, 2), lambda: b_row(3, 2), c_wo.wait, g_wo.start_z],
        4: [lambda: b_row(1, 3), lambda: b_row(3, 3)],
        5: [lambda: b_row(1, 4), lambda: b_row(3, 4), lambda: far_row(0)],
        6: [lambda: b_row(1, 5), lambda: b_row(3, 5), lambda: far_row(1)],
        7: [lambda: b_row(1, 6), lambda: b_row(3, 6), lambda: far_row(2)],
        8: [lambda: b_row(1, 7), lambda: b_row(3, 7), lambda: far_row(3)],
        9: [lambda: far_row(4), g_wo.start_x],
        10: [lambda: far_row(5)],
        11: [lambda: far_row(6), lambda: far_row(7)],
        13: [g_wo.start_far],
    }
    for j, (ref, b, h) in enumerate(groups):
        for event in events.get(j, ()):
            event()
        if ref is koth:
            got(koth.at[b, pl.ds(4 * h, 4)], r_d.at[2 * b + h])
        score(ref, b, h, j % 2)
        if j > 0:
            weigh((j - 1) % 2, j == 1)
    weigh((len(groups) - 1) % 2, False)

    head_lane = lax.broadcasted_iota(jnp.int32, (block, nk), 1) // VDIM
    attended = jnp.zeros((block, nk), F32)
    sums = []
    for head in range(heads):
        rows = pl.ds(head * block, block)
        weight_sum = jnp.sum(sum_s[rows, :], axis=-1, keepdims=True)
        attended = jnp.where(head_lane == head, acc_s[rows, :] / weight_sum, attended)
        log_sum = jnp.broadcast_to(top_s[rows, :1] * math.log(2.0) + jnp.log(weight_sum), (block, block))
        sums.append(jnp.sum(jnp.where(down == across, log_sum, 0.0), axis=0, keepdims=True))
    log_out[...] = jnp.concatenate(sums, axis=0)
    att[...] = attended.astype(BF16)

    g_wo.finish()
    whole = dot_t(att[...], wo[...].reshape(width, nk))
    prod[...] = whole.reshape(NY, 2, own, width)

    def f_c(k):
        return rc(part.at[k], got_core.at[k], s_f.at[0], r_f.at[k], c_dev)

    def f_y(k):
        return rc(send_y.at[k], got_y.at[k], s_f.at[1], r_f.at[NY + k], dev(dy=k))

    order = (2, 1, 3, 0)
    for k in order:
        part[k] = prod[wrap(y + k, NY), 1 - core].astype(BF16)
        f_c(k).start()
    for k in order[:-1]:
        far = prod[wrap(y + k, NY), core]
        f_c(k).wait_recv()
        send_y[k] = (far + got_core[k].astype(F32)).astype(BF16)
        f_y(k).start()
    near = prod[y, core]
    f_c(0).wait_recv()
    near = near + got_core[0].astype(F32)
    c_out.wait()
    for k in (1, 3, 2):
        f_y(k).wait_recv()
        near = near + got_y[k].astype(F32)
    out[...] = rms(near.astype(BF16), gain_out[...])

    for gather in (g_k, g_up, g_uq, g_wo):
        gather.drain()
    sent(tok.at[core], s_tok.at[0])
    sent(kown.at[0, pl.ds(0, 7)], s_z.at[0])
    sent(kown.at[pl.ds(0, 3)], s_b.at[0])
    sent(kown, s_d.at[0])
    sent(part, s_f.at[0])
    sent(send_y.at[pl.ds(1, 3)], s_f.at[1])

    @pl.when(core == 0)
    def _():
        g_wr.drain()
        sent(kown.at[0, 0, pl.ds(0, 3)], s_a.at[0])
        sent(kown.at[0, 0], s_a.at[1])

    @pl.when(core == 1)
    def _():
        sent(ql, s_q.at[0])
        sent(ql.at[pl.ds(0, 3)], s_q.at[1])


def on_device(n, ntp, tokens, doc_ids, down_q, down_k, down_r, gain_q, gain_k, up_q, up_k, up_v, out_w, gain_o):
    own, width = tokens.shape
    block = doc_ids.shape[0]
    heads = up_k.shape[1] // NOPE
    rank = down_k.shape[1]
    nq, nk, nv = up_q.shape[1], up_k.shape[1], up_v.shape[1]
    turn_in, turn_block, pick, pick_key = tables(n, block, heads)
    vmem = pl.BlockSpec(memory_space=pltpu.VMEM)
    hbm = pl.BlockSpec(memory_space=pl.ANY)
    dma = lambda k: pltpu.SemaphoreType.DMA((k,))
    v = lambda *shape, dtype=BF16: pltpu.VMEM(shape, dtype)
    rows = heads * block
    scratch = [
        pltpu.VMEM((1, block), jnp.int32), v(1, rank, dtype=F32), v(1, width, dtype=F32), v(1, 256, dtype=F32), v(ROPE, 256),
        v(2, own, width), v(NZ, NX, width // n, rank), v(NZ, NX, width // n, ROPE),
        v(NZ, NX, rank // n, nq), v(NZ, NX, rank // n, nk + nv), v(NZ, NX, width // n, nv),
        v(rank, nq), v(rank, nk + nv), v(NY, 2 * own, rank),
        v(4, NZ, 4, 5, own // 2, 128), v(4, NZ, 4, 5, own // 2, 128), v(5, own // 2, 128),
        v(block, 256, dtype=F32), v(block, 128, dtype=F32), v(block, 128, dtype=F32), v(*pick.shape),
        v(2, rows, 256),
        v(2, 2, rows, 256, dtype=F32), v(2, 512, nv),
        v(rows, 128, dtype=F32), v(rows, 128, dtype=F32), v(rows, 128, dtype=F32),
        v(block, nv), v(NY, 2, own, width, dtype=F32),
        v(NY, own, width), v(NY, own, width), v(NY, own, width), v(NY, own, width),
        dma(14), dma(1), dma(1), dma(2), dma(24), dma(2), dma(4), dma(2), dma(4), dma(2), dma(4), dma(2), dma(4),
        dma(2), dma(1), dma(2), dma(1), dma(1), dma(8), dma(1), dma(32), dma(1), dma(8), dma(2), dma(8),
    ]
    mixed, log_sums = pl.pallas_call(
        functools.partial(kernel, n, ntp, heads),
        out_shape=(
            jax.ShapeDtypeStruct((own, width), BF16),
            jax.ShapeDtypeStruct((heads, block), F32),
        ),
        in_specs=[hbm] * 16,
        out_specs=(vmem, vmem),
        scratch_shapes=scratch,
        compiler_params=pltpu.CompilerParams(
            collective_id=0, has_side_effects=True, vmem_limit_bytes=60 * 1024 * 1024
        ),
    )(
        tokens, doc_ids[None, :], down_q, down_k, down_r, gain_q[None, :], gain_k[None, :],
        up_q, up_k, up_v, out_w.T, gain_o[None, :],
        jnp.asarray(turn_in), jnp.asarray(turn_block[:, None, :]), jnp.asarray(pick, BF16), jnp.asarray(pick_key, BF16),
    )
    return mixed, log_sums.T


def solution(mesh):
    assert mesh.shape["tp"] == 2 * NY and mesh.shape["sp"] == NX * NZ
    placed = (
        P(("sp", "tp"), None), P("sp"), P("sp", None), P("sp", None), P("sp", None), P(), P(),
        P("sp", "tp"), P("sp", "tp"), P("sp", "tp"), P("tp", "sp"), P(),
    )
    return jax.shard_map(
        functools.partial(on_device, mesh.shape["sp"], mesh.shape["tp"]),
        mesh=mesh,
        in_specs=placed,
        out_specs=(P(("sp", "tp"), None), P("sp", "tp")),
        check_vma=False,
    )
```

time: 69.9 us -> 68.4 us (0.979)
  Pallas kernels: 66.9 us -> 65.5 us
    pallas_call x1 -> x0, local copies, waits for them, and re-layouts: 1.59 us -> none  [on_device(): pl.pallas_call(functools.partial(kernel, n, ntp, heads), out_shape=(jax.S...]
    unnamed x3 -> x4, local copies, waits for them, and re-layouts: 0.63 us -> 2.06 us
    pallas_call x1, Pallas kernels: 66.9 us -> 65.5 us  [on_device(): pl.pallas_call(functools.partial(kernel, n, ntp, heads), out_shape=(jax.S...]
where the time goes in v2:
time: 68.4 us; the launch traced here: 68.3 us
  Pallas kernels  65.5 us (96%)
  local copies, waits for them, and re-layouts  2.06 us (3%)
    pallas_call x1, Pallas kernels, on_device(): pl.pallas_call(functools.partial(kernel, n, ntp, heads), out_shape=(jax.S...  65.5 us
    unnamed x4, local copies, waits for them, and re-layouts  2.06 us

profile of v2, /device:TPU:1, one launch (start us, length us, event | category | flops | bytes accessed | tf_op | source)
XLA Modules:
  0.0 68.3 jit_solution(16160960595792281302)
XLA Ops:
  0.6 65.5 %shard_map.167 = (bf16[32,1024]{1,0:T(8,128)(2,1)}, f32[2,256]{1,0:T(2,128)}) custom-call(bf16[32,1024]{1,0:T(8,128)(2,1)} %tokens.1, s32[1,256]{1,0:T(1,128)} %bitcast.9, bf16[32,256]{1,0:T(8,128)(2,1)} %down_q.1, bf16[32,256]{1,0:T(8,128)(2,1)} %down_k.1, bf16[32,32]{1,0:T(8,128)(2,1)} %down_r.1, f32[1,256]{1,0:T(1,128)} %bitcast.10, f32[1,256]{1,0:T(1,128)} %bitcast.11, ...), custom_call_target="tpu_custom_call" | custom-call | tf_op jit(solution)/shard_map/pallas_call | solution.py:556
  66.2 0.0 copy-start
  66.2 1.5 %copy.20 = bf16[32,1024]{1,0:T(8,128)(2,1)} copy(bf16[32,1024]{1,0:T(8,128)(2,1)} %get-tuple-element.8) | data formatting | bytes 131072
  67.7 0.0 copy-done
  67.7 0.6 copy.21
Async XLA Ops:
  66.2 1.5 %copy-start = (f32[2,256]{1,0:T(2,128)S(1)}, f32[2,256]{1,0:T(2,128)}, u32[]{:S(2)}) copy-start(f32[2,256]{1,0:T(2,128)} %get-tuple-element.5) | copy-start | bytes 6148

commit v3 on v2

--- a/solution.py
+++ b/solution.py
@@ -63,18 +63,21 @@
     pick_key[rot, rot] = 1
     pick_key[half + low, 128 + low] = -1
     pick_key[low, 128 + half + low] = 1
-    return turn(np.arange(block)), turn(np.arange(n) * block), pick, pick_key
+    mix = np.zeros((128, 128), np.float32)
+    to = np.arange(128)
+    mix[32 * (to // 8 % 4) + 8 * (to // 32) + to % 8, to] = 1
+    return turn(np.arange(block)), turn(np.arange(n) * block), pick, pick_key, mix
 
 
 def kernel(
     n, ntp, heads,
     tokens, docs_in, down_q, down_k, down_r, gain_q, gain_k, up_q, up_k, up_v, out_wt, gain_o,
-    turn_in, turn_block, pick, pick_key,
+    turn_in, turn_block, pick, pick_key, mix,
     out, log_out,
-    docs, gain, gain_out, turn_me, sel_key,
+    docs, gain, gain_out, turn_me, sel_key, mix_in, tok_mix, wr_in, wr_flat,
     tok, w, wr, uq, up, wo, uq_flat, up_flat, ql, kown, koth, ks, tab, kdoc, qdoc, sel, qs,
-    sbuf, vbuf, top_s, sum_s, acc_s, att, prod, part, got_core, got_y, send_y,
-    loc, s_tok, r_tok, s_w, r_w, s_wr, r_wr, s_uq, r_uq, s_up, r_up, s_wo, r_wo,
+    sbuf, kbuf, vbuf, top_s, sum_s, acc_s, att, prod, part, got_core, got_y, send_y,
+    go, loc, s_tok, r_tok, s_w, r_w, s_wr, r_wr, s_uq, r_uq, s_up, r_up, s_wo, r_wo,
     s_q, r_q, s_a, r_a, s_z, r_z, s_b, r_b, s_d, r_d, s_f, r_f,
 ):
     me = lax.axis_index("sp")
@@ -118,12 +121,12 @@
     for device in others:
         pl.semaphore_signal(barrier, inc=1, device_id=device, device_id_type=MESH)
 
-    @pl.when(core == 0)
+    @pl.when(core == 1)
     def _():
         pltpu.make_async_copy(down_k, w.at[z, x], loc.at[1]).start()
         pltpu.make_async_copy(gain_k, gain, loc.at[9]).start()
 
-    @pl.when(core == 1)
+    @pl.when(core == 0)
     def _():
         pltpu.make_async_copy(down_q, w.at[z, x], loc.at[1]).start()
         pltpu.make_async_copy(gain_q, gain, loc.at[9]).start()
@@ -135,7 +138,8 @@
     c_tab = pltpu.make_async_copy(turn_in, tab, loc.at[7])
     c_me = pltpu.make_async_copy(turn_block.at[me], turn_me, loc.at[11])
     c_tok = pltpu.make_async_copy(tokens, tok.at[core], loc.at[0])
-    c_wr = pltpu.make_async_copy(down_r, wr.at[z, x], loc.at[2])
+    c_wr = pltpu.make_async_copy(down_r, wr_in, loc.at[2])
+    c_mix = pltpu.make_async_copy(mix, mix_in, loc.at[14])
     c_uq = pltpu.make_async_copy(up_q, uq.at[z, x], loc.at[3])
     c_up = [
         pltpu.make_async_copy(up_k, up.at[z, x, :, pl.ds(0, nk)], loc.at[4]),
@@ -145,7 +149,7 @@
     c_sel = pltpu.make_async_copy(pick, sel, loc.at[8])
     c_key = pltpu.make_async_copy(pick_key, sel_key, loc.at[12])
     c_out = pltpu.make_async_copy(gain_o, gain_out, loc.at[13])
-    for copy in [c_docs, c_tab, c_me, c_wr, c_tok, c_uq] + c_up + [c_key, c_wo, c_sel, c_out]:
+    for copy in [c_docs, c_tab, c_me, c_wr, c_tok, c_uq] + c_up + [c_key, c_mix, c_wo, c_sel, c_out]:
         copy.start()
 
     down = lax.broadcasted_iota(jnp.int32, (block, block), 0)
@@ -165,131 +169,112 @@
     tab[:, :128] = cos_a * cos_b - sin_a * sin_b
     tab[:, 128:] = sin_a * cos_b + cos_a * sin_b
 
-    for copy in [c_w, c_wr, c_tok, c_uq] + c_up + [c_key, c_gain]:
+    rank = uq_flat.shape[0]
+    c_wr.wait()
+    wide_r = wr_in[...].astype(F32)
+    wr[z, x] = jnp.concatenate([wide_r[8 * q : 8 * q + 8] for q in range(4)], axis=1)
+    for copy in [c_w, c_tok, c_uq] + c_up + [c_key, c_mix, c_gain]:
         copy.wait()
     pl.semaphore_wait(barrier, len(others))
 
-    class Batch:
+    class Gather:
         def __init__(self, ref, s, r):
             self.ref, self.s, self.r = ref, s, r
 
         def start_z(self):
             here = self.ref.at[z, x]
-            for d in NEAR[1:]:
+            for d in reversed(NEAR[1:]):
                 rc(here, here, self.s.at[0], self.r.at[0], dev(dz=d)).start()
 
         def start_x(self):
             got(self.ref.at[pl.ds(0, NZ - 1), x], self.r.at[0])
             column = self.ref.at[:, x]
-            rc(column, column, self.s.at[1], self.r.at[1], dev(dx=1)).start()
-            rc(column, column, self.s.at[1], self.r.at[2], dev(dx=-1)).start()
-
-        def start_far(self):
-            got(self.ref.at[:, wrap(x - 1, NX)], self.r.at[1])
-            low = self.ref.at[pl.ds(0, NZ // 2), wrap(x - 1, NX)]
-            rc(low, low, self.s.at[1], self.r.at[3], dev(dx=1)).start()
-            got(self.ref.at[:, wrap(x + 1, NX)], self.r.at[2])
-            high = self.ref.at[pl.ds(NZ // 2, NZ // 2), wrap(x + 1, NX)]
-            rc(high, high, self.s.at[1], self.r.at[3], dev(dx=-1)).start()
+            for k in (2, 1, -1):
+                rc(column, column, self.s.at[1], self.r.at[1], dev(dx=k)).start()
 
         def finish(self):
-            got(self.ref.at[:, wrap(x + 2, NX)], self.r.at[3])
+            got(self.ref.at[pl.ds(0, NZ - 2)], self.r.at[1])
 
         def drain(self):
-            sent(self.ref.at[pl.ds(0, NZ - 1), x], self.s.at[0])
+            sent(self.ref.at[pl.ds(0, NZ - 1), 0], self.s.at[0])
             sent(self.ref.at[pl.ds(0, NZ - 2)], self.s.at[1])
 
-    class Pieces(Batch):
+    class Pieces(Gather):
         def start_z(self):
             here = self.ref.at[z, x]
-            for d in NEAR[1:]:
+            for d in reversed(NEAR[1:]):
                 rc(here, here, self.s.at[0], self.r.at[d], dev(dz=d)).start()
 
-        def x_of(self, d):
+        def pass_x(self, d):
             here = self.ref.at[wrap(z - d, NZ), x]
             if d > 0:
                 got(here, self.r.at[d])
-            rc(here, here, self.s.at[1], self.r.at[8 + d], dev(dx=1)).start()
-            rc(here, here, self.s.at[1], self.r.at[16 + d], dev(dx=-1)).start()
-
-        def far_of(self, d):
-            low = self.ref.at[wrap(z - d, NZ), wrap(x - 1, NX)]
-            high = self.ref.at[wrap(z - d, NZ), wrap(x + 1, NX)]
-            got(low, self.r.at[8 + d])
-            if d in (0, 7, 6, 5):
-                rc(low, low, self.s.at[1], self.r.at[0], dev(dx=1)).start()
-            got(high, self.r.at[16 + d])
-            if d in (1, 2, 3, 4):
-                rc(high, high, self.s.at[1], self.r.at[0], dev(dx=-1)).start()
+            for k in (2, 1, -1):
+                rc(here, here, self.s.at[1], self.r.at[0], dev(dx=k)).start()
 
         def finish(self):
-            got(self.ref.at[:, wrap(x + 2, NX)], self.r.at[0])
+            got(self.ref.at[pl.ds(0, NZ - 2)], self.r.at[0])
 
     g_k = Pieces(w, s_w, r_w)
-    g_q = Batch(w, s_w, r_w)
-    g_wr = Batch(wr, s_wr, r_wr)
-    g_uq = Batch(uq, s_uq, r_uq)
-    g_up = Batch(up, s_up, r_up)
-    g_wo = Batch(wo, s_wo, r_wo)
+    g_wr = Pieces(wr, s_wr, r_wr)
+    g_q = Gather(w, s_w, r_w)
+    g_uq = Gather(uq, s_uq, r_uq)
+    g_up = Gather(up, s_up, r_up)
+    g_wo = Gather(wo, s_wo, r_wo)
     here = tok.at[core]
     c_partner = rc(here, here, s_tok.at[0], r_tok.at[0], c_dev)
 
-    @pl.when(core == 0)
+    @pl.when(core == 1)
     def _():
         g_k.start_z()
-        g_k.x_of(0)
         g_wr.start_z()
+        g_k.pass_x(0)
+        g_wr.pass_x(0)
         c_partner.start()
+        for d in NEAR[1:]:
+            g_k.pass_x(d)
+            g_wr.pass_x(d)
+            if d == 6:
+                pl.semaphore_signal(go, inc=1, device_id=c_dev, device_id_type=MESH)
         g_up.start_z()
         g_uq.start_z()
-        for d in (1, 7, 2, 6):
-            g_k.x_of(d)
-        g_k.far_of(0)
-        for d in (3, 5):
-            g_k.x_of(d)
-        g_k.far_of(1)
-        g_k.far_of(7)
-        g_k.x_of(4)
-        g_wr.start_x()
-        for d in (2, 6, 3, 5, 4):
-            g_k.far_of(d)
-        g_wr.start_far()
-
-    @pl.when(core == 1)
-    def _():
+        got(tok.at[1 - core], r_tok.at[0])
+        both_tokens = tok[...].reshape(2 * own, width)
+        for j in range(width // 128):
+            cut = slice(j * 128, (j + 1) * 128)
+            tok_mix[:, cut] = dot(both_tokens[:, cut], mix_in[...]).astype(BF16)
+        g_wr.finish()
+        packed = wr[...].reshape(rank, 128)
+        for q in range(4):
+            turned = (pltpu.roll(packed, 128 - 32 * q, 1) if q else packed).astype(BF16)
+            for j in range(width // 128):
+                wr_flat[j * 128 + q * 32 : j * 128 + (q + 1) * 32, :] = turned[j * 32 : (j + 1) * 32]
+        g_k.finish()
+
+    @pl.when(core == 0)
+    def _():
+        c_partner.start()
+        pl.semaphore_wait(go, 1)
         g_q.start_z()
-        c_partner.start()
         g_up.start_z()
         g_uq.start_z()
         g_q.start_x()
-        g_q.start_far()
-
-    g_up.start_x()
-    g_uq.start_x()
-    got(tok.at[1 - core], r_tok.at[0])
-
-    @pl.when(core == 0)
-    def _():
-        g_k.finish()
-        g_wr.finish()
+        g_up.start_x()
+        g_uq.start_x()
+    def project():
+        raw = dot(tok[...].reshape(2 * own, width), w[...].reshape(width, w.shape[-1])).astype(BF16)
+        return rms(raw, gain[...])
 
     @pl.when(core == 1)
     def _():
-        g_q.finish()
-
-    chip_tokens = tok[...].reshape(2 * own, width)
-    raw = dot(chip_tokens, w[...].reshape(width, w.shape[-1])).astype(BF16)
-    lat = rms(raw, gain[...])
-
-    @pl.when(core == 0)
-    def _():
-        rotary = dot(chip_tokens, wr[...].reshape(width, ROPE)).astype(BF16)
+        lat = project()
+        rotary = dot(tok_mix[...], wr_flat[...])[:, :ROPE].astype(BF16)
         both = dot(rotary, sel_key[...])
         rows = pl.ds(pl.multiple_of(y * (2 * own), 2 * own), 2 * own)
         turned = both[:, :128] * tab[rows, :128] + both[:, 128:] * tab[rows, 128:] + kdoc[rows, :]
+        half = own // 2
         for stripe in range(2):
             first = stripe * own
-            half = own // 2
             parts = [
                 lat[first + s * half : first + (s + 1) * half, h * 128 : (h + 1) * 128]
                 for s in range(2)
@@ -298,25 +283,18 @@
             packed = turned[first : first + half] + pltpu.roll(turned[first + half : first + own], 64, 1)
             parts.append(packed.astype(BF16))
             for i, tile in enumerate(parts):
-                if stripe == 0:
+                if stripe == 1:
                     kown[0, 0, 0, i] = tile
                 else:
                     ks[i] = tile
         here = kown.at[0, 0, 0]
-        rc(ks, here, s_a.at[1], r_a.at[0], dev(c=1)).start()
+        rc(ks, here, s_a.at[1], r_a.at[0], dev(c=0)).start()
         for k in (2, 1, 3):
             there = kown.at[0, 0, (-k) % 4]
-            rc(here, there, s_a.at[0], r_a.at[0], dev(dx=k)).start()
-            rc(ks, there, s_a.at[1], r_a.at[0], dev(dy=k, c=1)).start()
-
-    @pl.when(core == 1)
-    def _():
-        ql[y] = lat
-        here = ql.at[y]
-        for k in (2, 1, 3):
-            for c in range(2):
-                rc(here, here, s_q.at[c], r_q.at[0], dev(dy=k, c=c)).start()
-        rc(here, here, s_q.at[0], r_q.at[0], dev(c=0)).start()
+            rc(ks, there, s_a.at[1], r_a.at[0], dev(dx=k, c=0)).start()
+            rc(here, there, s_a.at[0], r_a.at[0], dev(dy=k)).start()
+        g_up.start_x()
+        g_uq.start_x()
 
     def z_send(src_pos, d, total, pieces=None):
         pos = ZPOS[(-total) % NZ]
@@ -331,11 +309,11 @@
         rc(kown.at[b, pos], koth.at[b, pos], s_d.at[0], r_d.at[2 * b + pos // 4], c_dev).start()
 
     def first_row():
-        @pl.when(core == 0)
+        @pl.when(core == 1)
         def _():
             got(kown.at[0, 0, pl.ds(1, 3)], r_a.at[0])
 
-        @pl.when(core == 1)
+        @pl.when(core == 0)
         def _():
             got(kown.at[0, 0], r_a.at[0])
 
@@ -371,19 +349,31 @@
         d_send(2, pos)
 
     first_row()
-    g_up.start_far()
-    g_uq.start_far()
+
+    @pl.when(core == 0)
+    def _():
+        got(tok.at[1 - core], r_tok.at[0])
+        g_q.finish()
+        ql[y] = project()
+        here = ql.at[y]
+        for k in (2, 1, 3):
+            for c in range(2):
+                rc(here, here, s_q.at[c], r_q.at[0], dev(dy=k, c=c)).start()
+        rc(here, here, s_q.at[1], r_q.at[0], dev(c=1)).start()
+
+    for pos in (1, 2, 3, 4):
+        z_row(pos)
     g_up.finish()
     g_uq.finish()
     for j in range(n):
         up_flat[j * 8 : (j + 1) * 8, :] = up[j // NX, j % NX]
         uq_flat[j * 8 : (j + 1) * 8, :] = uq[j // NX, j % NX]
 
+    @pl.when(core == 1)
+    def _():
+        got(ql, r_q.at[0])
+
     @pl.when(core == 0)
-    def _():
-        got(ql, r_q.at[0])
-
-    @pl.when(core == 1)
     def _():
         got(ql.at[pl.ds(0, 3)], r_q.at[0])
 
@@ -401,19 +391,27 @@
         qs[0, rows, 128:] = turned.astype(BF16)
         qs[1, rows, 128:] = pltpu.roll(turned, 64, 1).astype(BF16)
 
-    def score(ref, b, h, par):
+    def tiles(ref, b, h, i):
+        return ref[b, 4 * h : 4 * h + 4, :, i].reshape(256, 128)
+
+    def expand(j):
+        ref, b, h = groups[j]
         for s in range(2):
-            def tiles(i):
-                return ref[b, 4 * h : 4 * h + 4, :, i].reshape(256, 128)
-
-            kv = dot(jnp.concatenate([tiles(2 * s), tiles(2 * s + 1)], axis=1), up_flat[...]).astype(BF16)
-            keys = jnp.concatenate([kv[:, :nk], tiles(4)], axis=1)
-            vbuf[par, s * 256 : (s + 1) * 256, :] = kv[:, nk:]
-            sbuf[par, s] = dot_t(qs[s], keys)
+            lat = jnp.concatenate([tiles(ref, b, h, 2 * s), tiles(ref, b, h, 2 * s + 1)], axis=1)
+            kv = dot(lat, up_flat[...]).astype(BF16)
+            kbuf[j % 2, s] = kv[:, :nk]
+            vbuf[j % 3, s * 256 : (s + 1) * 256, :] = kv[:, nk:]
+
+    def score(j):
+        ref, b, h = groups[j]
+        rot = tiles(ref, b, h, 4)
+        for s in range(2):
+            sbuf[j % 2, s] = dot_t(qs[s], jnp.concatenate([kbuf[j % 2, s], rot], axis=1))
 
     step = 128
 
-    def weigh(par, first):
+    def weigh(j):
+        par, first = j % 2, j == 0
         for r in range(0, rows_all, step):
             rows = pl.ds(r, step)
             parts = [sbuf[par, s, rows, h * 128 : (h + 1) * 128] for s in range(2) for h in range(2)]
@@ -427,7 +425,7 @@
                 alpha = jnp.exp2(old - new)
             weights = [jnp.exp2(p - new) for p in parts]
             total = (weights[0] + weights[1]) + (weights[2] + weights[3])
-            mixed = dot(jnp.concatenate([p.astype(BF16) for p in weights], axis=1), vbuf[par])
+            mixed = dot(jnp.concatenate([p.astype(BF16) for p in weights], axis=1), vbuf[j % 3])
             top_s[rows, :] = new
             if first:
                 sum_s[rows, :] = total
@@ -441,7 +439,6 @@
         groups.append((kown, b, h))
         groups.append((koth, b, h))
     events = {
-        0: [lambda p=p: z_row(p) for p in (1, 2, 3, 4)],
         1: [lambda: b_row(1, 0), lambda: b_row(3, 0), lambda: z_row(5), lambda: z_row(6)],
         2: [lambda: z_row(7), lambda: b_row(1, 1), lambda: b_row(3, 1)],
         3: [lambda: b_row(1, 2), lambda: b_row(3, 2), c_wo.wait, g_wo.start_z],
@@ -453,17 +450,21 @@
         9: [lambda: far_row(4), g_wo.start_x],
         10: [lambda: far_row(5)],
         11: [lambda: far_row(6), lambda: far_row(7)],
-        13: [g_wo.start_far],
     }
     for j, (ref, b, h) in enumerate(groups):
         for event in events.get(j, ()):
             event()
         if ref is koth:
             got(koth.at[b, pl.ds(4 * h, 4)], r_d.at[2 * b + h])
-        score(ref, b, h, j % 2)
-        if j > 0:
-            weigh((j - 1) % 2, j == 1)
-    weigh((len(groups) - 1) % 2, False)
+        expand(j)
+        if j >= 1:
+            score(j - 1)
+        if j >= 2:
+            weigh(j - 2)
+    last = len(groups) - 1
+    score(last)
+    weigh(last - 1)
+    weigh(last)
 
     head_lane = lax.broadcasted_iota(jnp.int32, (block, nk), 1) // VDIM
     attended = jnp.zeros((block, nk), F32)
@@ -505,7 +506,7 @@
         near = near + got_y[k].astype(F32)
     out[...] = rms(near.astype(BF16), gain_out[...])
 
-    for gather in (g_k, g_up, g_uq, g_wo):
+    for gather in (g_up, g_uq, g_wo):
         gather.drain()
     sent(tok.at[core], s_tok.at[0])
     sent(kown.at[0, pl.ds(0, 7)], s_z.at[0])
@@ -514,16 +515,18 @@
     sent(part, s_f.at[0])
     sent(send_y.at[pl.ds(1, 3)], s_f.at[1])
 
-    @pl.when(core == 0)
-    def _():
+    @pl.when(core == 1)
+    def _():
+        g_k.drain()
         g_wr.drain()
         sent(kown.at[0, 0, pl.ds(0, 3)], s_a.at[0])
         sent(kown.at[0, 0], s_a.at[1])
 
-    @pl.when(core == 1)
-    def _():
-        sent(ql, s_q.at[0])
-        sent(ql.at[pl.ds(0, 3)], s_q.at[1])
+    @pl.when(core == 0)
+    def _():
+        g_q.drain()
+        sent(ql, s_q.at[1])
+        sent(ql.at[pl.ds(0, 3)], s_q.at[0])
 
 
 def on_device(n, ntp, tokens, doc_ids, down_q, down_k, down_r, gain_q, gain_k, up_q, up_k, up_v, out_w, gain_o):
@@ -532,7 +535,7 @@
     heads = up_k.shape[1] // NOPE
     rank = down_k.shape[1]
     nq, nk, nv = up_q.shape[1], up_k.shape[1], up_v.shape[1]
-    turn_in, turn_block, pick, pick_key = tables(n, block, heads)
+    turn_in, turn_block, pick, pick_key, mix = tables(n, block, heads)
     vmem = pl.BlockSpec(memory_space=pltpu.VMEM)
     hbm = pl.BlockSpec(memory_space=pl.ANY)
     dma = lambda k: pltpu.SemaphoreType.DMA((k,))
@@ -540,17 +543,19 @@
     rows = heads * block
     scratch = [
         pltpu.VMEM((1, block), jnp.int32), v(1, rank, dtype=F32), v(1, width, dtype=F32), v(1, 256, dtype=F32), v(ROPE, 256),
-        v(2, own, width), v(NZ, NX, width // n, rank), v(NZ, NX, width // n, ROPE),
+        v(128, 128), v(2 * own, width), v(width // n, ROPE), v(width, 128),
+        v(2, own, width), v(NZ, NX, width // n, rank), v(NZ, NX, width // n // 4, 128, dtype=F32),
         v(NZ, NX, rank // n, nq), v(NZ, NX, rank // n, nk + nv), v(NZ, NX, width // n, nv),
         v(rank, nq), v(rank, nk + nv), v(NY, 2 * own, rank),
         v(4, NZ, 4, 5, own // 2, 128), v(4, NZ, 4, 5, own // 2, 128), v(5, own // 2, 128),
         v(block, 256, dtype=F32), v(block, 128, dtype=F32), v(block, 128, dtype=F32), v(*pick.shape),
         v(2, rows, 256),
-        v(2, 2, rows, 256, dtype=F32), v(2, 512, nv),
+        v(2, 2, rows, 256, dtype=F32), v(2, 2, 256, nk), v(3, 512, nv),
         v(rows, 128, dtype=F32), v(rows, 128, dtype=F32), v(rows, 128, dtype=F32),
         v(block, nv), v(NY, 2, own, width, dtype=F32),
         v(NY, own, width), v(NY, own, width), v(NY, own, width), v(NY, own, width),
-        dma(14), dma(1), dma(1), dma(2), dma(24), dma(2), dma(4), dma(2), dma(4), dma(2), dma(4), dma(2), dma(4),
+        pltpu.SemaphoreType.REGULAR,
+        dma(15), dma(1), dma(1), dma(2), dma(8), dma(2), dma(8), dma(2), dma(2), dma(2), dma(2), dma(2), dma(2),
         dma(2), dma(1), dma(2), dma(1), dma(1), dma(8), dma(1), dma(32), dma(1), dma(8), dma(2), dma(8),
     ]
     mixed, log_sums = pl.pallas_call(
@@ -559,7 +564,7 @@
             jax.ShapeDtypeStruct((own, width), BF16),
             jax.ShapeDtypeStruct((heads, block), F32),
         ),
-        in_specs=[hbm] * 16,
+        in_specs=[hbm] * 17,
         out_specs=(vmem, vmem),
         scratch_shapes=scratch,
         compiler_params=pltpu.CompilerParams(
@@ -568,7 +573,7 @@
     )(
         tokens, doc_ids[None, :], down_q, down_k, down_r, gain_q[None, :], gain_k[None, :],
         up_q, up_k, up_v, out_w.T, gain_o[None, :],
-        jnp.asarray(turn_in), jnp.asarray(turn_block[:, None, :]), jnp.asarray(pick, BF16), jnp.asarray(pick_key, BF16),
+        jnp.asarray(turn_in), jnp.asarray(turn_block[:, None, :]), jnp.asarray(pick, BF16), jnp.asarray(pick_key, BF16), jnp.asarray(mix, BF16),
     )
     return mixed, log_sums.T
 

time: 68.4 us -> 59.7 us (0.87)
  Pallas kernels: 65.5 us -> 56.8 us
    pallas_call x1, Pallas kernels: 65.5 us -> 56.8 us  [on_device(): pl.pallas_call(functools.partial(kernel, n, ntp, heads), out_shape=(jax.S...]
where the time goes in v3:
time: 59.7 us; the launch traced here: 59.5 us
  Pallas kernels  56.8 us (95%)
  local copies, waits for them, and re-layouts  2.06 us (3%)
  between operations  0.65 us (1%)
    pallas_call x1, Pallas kernels, on_device(): pl.pallas_call(functools.partial(kernel, n, ntp, heads), out_shape=(jax.S...  56.8 us
    unnamed x4, local copies, waits for them, and re-layouts  2.06 us

profile of v3, /device:TPU:1, one launch (start us, length us, event | category | flops | bytes accessed | tf_op | source)
XLA Modules:
  0.0 59.5 jit_solution(2858249738854886377)
XLA Ops:
  0.6 56.8 %shard_map.176 = (bf16[32,1024]{1,0:T(8,128)(2,1)}, f32[2,256]{1,0:T(2,128)}) custom-call(bf16[32,1024]{1,0:T(8,128)(2,1)} %tokens.1, s32[1,256]{1,0:T(1,128)} %bitcast.9, bf16[32,256]{1,0:T(8,128)(2,1)} %down_q.1, bf16[32,256]{1,0:T(8,128)(2,1)} %down_k.1, bf16[32,32]{1,0:T(8,128)(2,1)} %down_r.1, f32[1,256]{1,0:T(1,128)} %bitcast.10, f32[1,256]{1,0:T(1,128)} %bitcast.11, ...), custom_call_target="tpu_custom_call" | custom-call | tf_op jit(solution)/shard_map/pallas_call | solution.py:561
  57.4 0.0 copy-start
  57.5 1.5 %copy.21 = bf16[32,1024]{1,0:T(8,128)(2,1)} copy(bf16[32,1024]{1,0:T(8,128)(2,1)} %get-tuple-element.8) | data formatting | bytes 131072
  58.9 0.0 copy-done
  58.9 0.6 copy.22
Async XLA Ops:
  57.4 1.5 %copy-start = (f32[2,256]{1,0:T(2,128)S(1)}, f32[2,256]{1,0:T(2,128)}, u32[]{:S(2)}) copy-start(f32[2,256]{1,0:T(2,128)} %get-tuple-element.5) | copy-start | bytes 6148

commit v4 on v3

v4 whole, which is shorter than its diff:
```python
import functools
import math

import jax
import jax.numpy as jnp
import numpy as np
from jax import lax
from jax.experimental import pallas as pl
from jax.experimental.pallas import tpu as pltpu
from jax.sharding import PartitionSpec as P

NOPE = 64
ROPE = 32
VDIM = 64
THETA = 10000.0
EPS = 1e-06
MASKED = -1e30
MESH = pl.DeviceIdType.MESH
F32 = jnp.float32
BF16 = jnp.bfloat16
NX, NY, NZ = 4, 4, 8
NEAR = (0, 1, 7, 2, 6, 3, 5, 4)
ZPOS = {rel: pos for pos, rel in enumerate(NEAR)}


def dot(a, b):
    return jnp.dot(a, b, preferred_element_type=F32)


def dot_t(a, b):
    return lax.dot_general(a, b, (((1,), (1,)), ((), ())), preferred_element_type=F32)


def rms(values, gain):
    wide = values.astype(F32)
    scale = lax.rsqrt(jnp.mean(wide * wide, axis=-1, keepdims=True) + EPS)
    return (wide * scale * gain).astype(BF16)


def tables(n, block, heads):
    half = ROPE // 2
    inverse = np.float32(THETA) ** (-np.arange(half, dtype=np.float32) / np.float32(half))
    inverse = inverse.astype(np.float32).astype(np.float64)[None, :]

    def turn(positions):
        angles = positions.astype(np.float64)[:, None] * inverse
        both = np.zeros((len(positions), 256), np.float32)
        both[:, :ROPE] = np.tile(np.cos(angles), (1, 2))
        both[:, 128 : 128 + ROPE] = np.tile(np.sin(angles), (1, 2))
        return both

    width = NOPE + ROPE
    pick = np.zeros((heads * width, heads * 384), np.float32)
    eye = np.arange(NOPE)
    rot = np.arange(ROPE)
    low = np.arange(half)
    for head in range(heads):
        pick[head * width + eye, head * 384 + (head % 2) * NOPE + eye] = 1
        pick[head * width + NOPE + rot, head * 384 + 128 + rot] = 1
        pick[head * width + NOPE + half + low, head * 384 + 256 + low] = -1
        pick[head * width + NOPE + low, head * 384 + 256 + half + low] = 1
    pick_key = np.zeros((ROPE, 256), np.float32)
    pick_key[rot, rot] = 1
    pick_key[half + low, 128 + low] = -1
    pick_key[low, 128 + half + low] = 1
    mix = np.zeros((128, 128), np.float32)
    to = np.arange(128)
    mix[32 * (to // 8 % 4) + 8 * (to // 32) + to % 8, to] = 1
    return turn(np.arange(block)), turn(np.arange(n) * block), pick, pick_key, mix


def kernel(
    n, ntp, heads,
    tokens, docs_in, down_q, down_k, down_r, gain_q, gain_k, up_q, up_k, up_v, out_wt, gain_o,
    turn_in, turn_block, pick, pick_key, mix,
    out, log_out,
    docs, gain, gain_out, turn_me, sel_key, mix_in, tok_mix, wr_in, wr_flat,
    tok, w, wr, uq, up, wo, uq_flat, up_flat, ql, kown, koth, ks, tab, kdoc, qdoc, sel, qs,
    sbuf, kbuf, vbuf, top_s, sum_s, acc_s, osend, oget, lget,
    go, loc, s_tok, r_tok, s_w, r_w, s_wr, r_wr, s_uq, r_uq, s_up, r_up, s_wo, r_wo,
    s_q, r_q, s_a, r_a, s_z, r_z, s_d, r_d, s_f, r_f,
):
    me = lax.axis_index("sp")
    t = lax.axis_index("tp")
    z, x = me // NX, lax.rem(me, NX)
    y, core = t // 2, lax.rem(t, 2)
    own, width = tokens.shape
    block = ntp * own
    rows_all = heads * block

    def wrap(v, size):
        return lax.rem(v + size, size)

    def dev(dz=0, dx=0, dy=0, c=None):
        c = core if c is None else c
        zz = wrap(z + dz, NZ) if dz else z
        xx = wrap(x + dx, NX) if dx else x
        yy = wrap(y + dy, NY) if dy else y
        return (zz * NX + xx, yy * 2 + c)

    c_dev = dev(c=1 - core)

    def rc(src, dst, s, r, device):
        return pltpu.make_async_remote_copy(
            src_ref=src, dst_ref=dst, send_sem=s, recv_sem=r, device_id=device, device_id_type=MESH
        )

    def sent(ref, s):
        rc(ref, ref, s, s, c_dev).wait_send()

    def got(ref, r):
        rc(ref, ref, r, r, c_dev).wait_recv()

    barrier = pltpu.get_barrier_semaphore()
    others = [dev(dz=d) for d in range(1, NZ)] + [dev(dx=d) for d in range(1, NX)]
    others += [dev(dz=d, c=1 - core) for d in range(1, NZ)]
    others += [dev(dy=d) for d in range(1, NY)] + [dev(dy=d, c=1 - core) for d in range(NY)]
    for device in others:
        pl.semaphore_signal(barrier, inc=1, device_id=device, device_id_type=MESH)

    @pl.when(core == 1)
    def _():
        pltpu.make_async_copy(down_k, w.at[z, x], loc.at[1]).start()
        pltpu.make_async_copy(gain_k, gain, loc.at[9]).start()

    @pl.when(core == 0)
    def _():
        pltpu.make_async_copy(down_q, w.at[z, x], loc.at[1]).start()
        pltpu.make_async_copy(gain_q, gain, loc.at[9]).start()

    nq, nk = up_q.shape[1], up_k.shape[1]
    c_w = pltpu.make_async_copy(down_k, w.at[z, x], loc.at[1])
    c_gain = pltpu.make_async_copy(gain_k, gain, loc.at[9])
    c_docs = pltpu.make_async_copy(docs_in, docs, loc.at[10])
    c_tab = pltpu.make_async_copy(turn_in, tab, loc.at[7])
    c_me = pltpu.make_async_copy(turn_block.at[me], turn_me, loc.at[11])
    c_tok = pltpu.make_async_copy(tokens, tok.at[core], loc.at[0])
    c_wr = pltpu.make_async_copy(down_r, wr_in, loc.at[2])
    c_mix = pltpu.make_async_copy(mix, mix_in, loc.at[14])
    c_uq = pltpu.make_async_copy(up_q, uq.at[0, z, x], loc.at[3])
    c_up = [
        pltpu.make_async_copy(up_k, up.at[0, z, x, :, pl.ds(0, nk)], loc.at[4]),
        pltpu.make_async_copy(up_v, up.at[0, z, x, :, pl.ds(nk, nk)], loc.at[5]),
    ]
    c_wo = pltpu.make_async_copy(out_wt, wo.at[y, core, z, x], loc.at[6])
    c_sel = pltpu.make_async_copy(pick, sel, loc.at[8])
    c_key = pltpu.make_async_copy(pick_key, sel_key, loc.at[12])
    c_out = pltpu.make_async_copy(gain_o, gain_out, loc.at[13])
    for copy in [c_docs, c_tab, c_me, c_wr, c_tok, c_uq] + c_up + [c_key, c_mix, c_wo, c_sel, c_out]:
        copy.start()

    down = lax.broadcasted_iota(jnp.int32, (block, block), 0)
    across = lax.broadcasted_iota(jnp.int32, (block, block), 1)
    c_docs.wait()
    doc_row = jnp.broadcast_to(docs[...].astype(F32), (block, block))
    doc_col = jnp.sum(jnp.where(down == across, doc_row, 0.0), axis=-1, keepdims=True)
    lane = lax.broadcasted_iota(jnp.int32, (block, 128), 1)
    in_docs = (lane >= ROPE) & (lane < ROPE + n)
    same = doc_col == (lane - ROPE).astype(F32)
    kdoc[...] = jnp.where(in_docs & same, 1.0, 0.0)
    qdoc[...] = jnp.where(in_docs & jnp.logical_not(same), MASKED, 0.0)
    c_tab.wait()
    c_me.wait()
    cos_a, sin_a = turn_me[:, :128], turn_me[:, 128:]
    cos_b, sin_b = tab[:, :128], tab[:, 128:]
    tab[:, :128] = cos_a * cos_b - sin_a * sin_b
    tab[:, 128:] = sin_a * cos_b + cos_a * sin_b

    rank = uq_flat.shape[1]
    c_wr.wait()
    wide_r = wr_in[...].astype(F32)
    wr[z, x] = jnp.concatenate([wide_r[8 * q : 8 * q + 8] for q in range(4)], axis=1)
    for copy in [c_w, c_tok, c_uq] + c_up + [c_key, c_mix, c_gain, c_wo]:
        copy.wait()
    pl.semaphore_wait(barrier, len(others))

    class Gather:
        def __init__(self, at, s, r):
            self.at, self.s, self.r = at, s, r

        def start_z(self):
            here = self.at(z, x)
            for d in reversed(NEAR[1:]):
                rc(here, here, self.s.at[0], self.r.at[0], dev(dz=d)).start()

        def start_x(self):
            got(self.at(pl.ds(0, NZ - 1), x), self.r.at[0])
            column = self.at(slice(None), x)
            for k in (2, 1, -1):
                rc(column, column, self.s.at[1], self.r.at[1], dev(dx=k)).start()

        def finish(self):
            got(self.at(pl.ds(0, NZ - 2), slice(None)), self.r.at[1])

        def drain(self):
            sent(self.at(pl.ds(0, NZ - 1), 0), self.s.at[0])
            sent(self.at(pl.ds(0, NZ - 2), slice(None)), self.s.at[1])

    class Pieces(Gather):
        def start_z(self):
            here = self.at(z, x)
            for d in reversed(NEAR[1:]):
                rc(here, here, self.s.at[0], self.r.at[d], dev(dz=d)).start()

        def pass_x(self, d):
            here = self.at(wrap(z - d, NZ), x)
            if d > 0:
                got(here, self.r.at[d])
            for k in (2, 1, -1):
                rc(here, here, self.s.at[1], self.r.at[0], dev(dx=k)).start()

        def finish(self):
            got(self.at(pl.ds(0, NZ - 2), slice(None)), self.r.at[0])

    g_k = Pieces(lambda i, j: w.at[i, j], s_w, r_w)
    g_wr = Pieces(lambda i, j: wr.at[i, j], s_wr, r_wr)
    g_q = Gather(lambda i, j: w.at[i, j], s_w, r_w)
    g_uq = Gather(lambda i, j: uq.at[0, i, j], s_uq, r_uq)
    g_up = Gather(lambda i, j: up.at[0, i, j], s_up, r_up)
    g_wo = Gather(lambda i, j: wo.at[:, core, i, j], s_wo, r_wo)

    def wo_y():
        here = wo.at[y, core, z, x]
        for k in (2, 1, 3):
            rc(here, here, s_wo.at[2], r_wo.at[2], dev(dy=k)).start()

    def wo_z():
        got(wo.at[pl.ds(0, 3), core, z, x], r_wo.at[2])
        g_wo.start_z()

    def wo_cross():
        g_wo.finish()
        here = wo.at[:, core]
        rc(here, here, s_wo.at[3], r_wo.at[3], c_dev).start()


    def heads_y(ref, g, s, r):
        g.finish()
        for k in (1, 3, 2):
            rel = -k % NY
            rc(ref.at[0], ref.at[rel], s.at[2], r.at[1 + rel], dev(dy=k)).start()

    def heads_in(rel):
        if rel:
            got(up.at[rel], r_up.at[1 + rel])
            got(uq.at[rel], r_uq.at[1 + rel])
        for j in range(n):
            up_flat[rel, j * 8 : (j + 1) * 8, :] = up[rel, j // NX, j % NX]
            uq_flat[rel, j * 8 : (j + 1) * 8, :] = uq[rel, j // NX, j % NX]

    here = tok.at[core]
    c_partner = rc(here, here, s_tok.at[0], r_tok.at[0], c_dev)

    @pl.when(core == 1)
    def _():
        g_k.start_z()
        g_wr.start_z()
        g_k.pass_x(0)
        g_wr.pass_x(0)
        c_partner.start()
        wo_y()
        g_up.start_z()
        g_uq.start_z()
        for d in NEAR[1:]:
            g_k.pass_x(d)
            g_wr.pass_x(d)
            if d == 6:
                pl.semaphore_signal(go, inc=1, device_id=c_dev, device_id_type=MESH)
        g_up.start_x()
        g_uq.start_x()
        wo_z()
        got(tok.at[1 - core], r_tok.at[0])
        both_tokens = tok[...].reshape(2 * own, width)
        for j in range(width // 128):
            cut = slice(j * 128, (j + 1) * 128)
            tok_mix[:, cut] = dot(both_tokens[:, cut], mix_in[...]).astype(BF16)
        g_wr.finish()
        packed = wr[...].reshape(rank, 128)
        for q in range(4):
            turned = (pltpu.roll(packed, 128 - 32 * q, 1) if q else packed).astype(BF16)
            for j in range(width // 128):
                wr_flat[j * 128 + q * 32 : j * 128 + (q + 1) * 32, :] = turned[j * 32 : (j + 1) * 32]
        g_k.finish()

    @pl.when(core == 0)
    def _():
        c_partner.start()
        wo_y()
        g_up.start_z()
        g_uq.start_z()
        pl.semaphore_wait(go, 1)
        g_q.start_z()
        g_up.start_x()
        g_uq.start_x()
        g_q.start_x()
        wo_z()

    def project():
        raw = dot(tok[...].reshape(2 * own, width), w[...].reshape(width, w.shape[-1])).astype(BF16)
        return rms(raw, gain[...])

    @pl.when(core == 1)
    def _():
        lat = project()
        rotary = dot(tok_mix[...], wr_flat[...])[:, :ROPE].astype(BF16)
        both = dot(rotary, sel_key[...])
        rows = pl.ds(pl.multiple_of(y * (2 * own), 2 * own), 2 * own)
        turned = both[:, :128] * tab[rows, :128] + both[:, 128:] * tab[rows, 128:] + kdoc[rows, :]
        half = own // 2
        for stripe in range(2):
            first = stripe * own
            parts = [
                lat[first + s * half : first + (s + 1) * half, h * 128 : (h + 1) * 128]
                for s in range(2)
                for h in range(2)
            ]
            packed = turned[first : first + half] + pltpu.roll(turned[first + half : first + own], 64, 1)
            parts.append(packed.astype(BF16))
            for i, tile in enumerate(parts):
                if stripe == 1:
                    kown[0, 0, i] = tile
                else:
                    ks[i] = tile
        here = kown.at[0, 0]
        rc(ks, here, s_z.at[1], r_z.at[2], dev(c=0)).start()
        for d in (4, 1, 7, 6, 2, 3, 5):
            pos = ZPOS[-d % NZ]
            there, sem = kown.at[0, pos], r_z.at[0 if pos < 4 else 1]
            rc(ks, there, s_z.at[1], sem, dev(dz=d, c=0)).start()
            rc(here, there, s_z.at[0], sem, dev(dz=d)).start()

    parts = ((0, 1), (1, 3), (4, 4))

    def a_send(p):
        first, length = parts[p]
        src = kown.at[0, pl.ds(first, length)]
        for k in (2, 1, 3):
            rel = -k % NX
            sem = r_a.at[0] if p == 0 else r_a.at[3 * p - 3 + rel]
            rc(src, kown.at[rel, pl.ds(first, length)], s_a.at[0], sem, dev(dx=k)).start()

    def cross(a, count, p):
        cut = pl.ds(*parts[p])
        src, dst = kown.at[pl.ds(a, count), cut], koth.at[pl.ds(a, count), cut]
        rc(src, dst, s_d.at[0], r_d.at[1 if p == 2 else 0], c_dev).start()

    def z_part(p):
        if p == 0:
            @pl.when(core == 0)
            def _():
                got(kown.at[0, 0], r_z.at[2])
        else:
            got(kown.at[0, pl.ds(*parts[p])], r_z.at[p - 1])
        a_send(p)
        cross(0, 1, p)

    def a_part(p):
        if p == 0:
            got(kown.at[pl.ds(1, 3), 0], r_a.at[0])
            cross(1, 3, 0)
        else:
            for rel in (1, 3, 2):
                got(kown.at[rel, pl.ds(*parts[p])], r_a.at[3 * p - 3 + rel])
                cross(rel, 1, p)

    z_part(0)

    @pl.when(core == 0)
    def _():
        got(tok.at[1 - core], r_tok.at[0])
        g_q.finish()
        ql[y] = project()
        here = ql.at[y]
        for k in (2, 1, 3):
            for c in range(2):
                rc(here, here, s_q.at[c], r_q.at[0], dev(dy=k, c=c)).start()
        rc(here, here, s_q.at[1], r_q.at[0], dev(c=1)).start()

    heads_y(up, g_up, s_up, r_up)
    heads_y(uq, g_uq, s_uq, r_uq)
    heads_in(0)
    a_part(0)
    z_part(1)
    z_part(2)
    a_part(1)
    g_wo.start_x()

    @pl.when(core == 1)
    def _():
        got(ql, r_q.at[0])

    @pl.when(core == 0)
    def _():
        got(ql.at[pl.ds(0, 3)], r_q.at[0])

    c_sel.wait()
    scale = 1.0 / math.sqrt(NOPE + ROPE)
    factor = scale * math.log2(math.e)

    def queries_of(rel):
        projected = dot(ql[...].reshape(block, ql.shape[-1]), uq_flat[rel]).astype(BF16)
        for head in range(heads):
            laid = dot(projected, sel[:, head * 384 : (head + 1) * 384])
            turned = (laid[:, 128:256] * tab[:, :128] + laid[:, 256:] * tab[:, 128:]) * factor + qdoc[...]
            plain = (laid[:, :128] * factor).astype(BF16)
            rows = pl.ds(head * block, block)
            qs[rel, 0, rows, :128] = plain
            qs[rel, 1, rows, :128] = plain
            qs[rel, 0, rows, 128:] = turned.astype(BF16)
            qs[rel, 1, rows, 128:] = pltpu.roll(turned, 64, 1).astype(BF16)

    def tiles(ref, h, i):
        return ref[:, 4 * h : 4 * h + 4, i].reshape(256, 128)

    def expand(j):
        ref, h, rel = groups[j]
        for s in range(2):
            lat = jnp.concatenate([tiles(ref, h, 2 * s), tiles(ref, h, 2 * s + 1)], axis=1)
            kv = dot(lat, up_flat[rel]).astype(BF16)
            kbuf[j % 2, s] = kv[:, :nk]
            vbuf[j % 3, s * 256 : (s + 1) * 256, :] = kv[:, nk:]

    def score(j):
        ref, h, rel = groups[j]
        rot = tiles(ref, h, 4)
        for s in range(2):
            sbuf[j % 2, s] = dot_t(qs[rel, s], jnp.concatenate([kbuf[j % 2, s], rot], axis=1))

    step = 128

    def weigh(j):
        par, first, pair = j % 2, j % 4 == 0, j // 4 % 2
        for r in range(0, rows_all, step):
            rows = pl.ds(r, step)
            parts = [sbuf[par, s, rows, h * 128 : (h + 1) * 128] for s in range(2) for h in range(2)]
            most = jnp.maximum(jnp.maximum(parts[0], parts[1]), jnp.maximum(parts[2], parts[3]))
            most = jnp.max(most, axis=-1, keepdims=True)
            if first:
                new = jnp.broadcast_to(most, (step, 128))
            else:
                old = top_s[pair, rows, :]
                new = jnp.maximum(old, most)
                alpha = jnp.exp2(old - new)
            weights = [jnp.exp2(p - new) for p in parts]
            total = (weights[0] + weights[1]) + (weights[2] + weights[3])
            mixed = dot(jnp.concatenate([p.astype(BF16) for p in weights], axis=1), vbuf[j % 3])
            top_s[pair, rows, :] = new
            if first:
                sum_s[pair, rows, :] = total
                acc_s[pair, rows, :] = mixed
            else:
                sum_s[pair, rows, :] = sum_s[pair, rows, :] * alpha + total
                acc_s[pair, rows, :] = acc_s[pair, rows, :] * alpha + mixed

    head_lane = lax.broadcasted_iota(jnp.int32, (block, nk), 1) // VDIM

    def close(i, rel):
        pair = i % 2
        outs, sums = [], []
        for head in range(heads):
            rows = pl.ds(head * block, block)
            weight_sum = jnp.sum(sum_s[pair, rows, :], axis=-1, keepdims=True)
            outs.append(acc_s[pair, rows, :] / weight_sum)
            log_sum = jnp.broadcast_to(top_s[pair, rows, :1] + jnp.log2(weight_sum), (block, block))
            sums.append(jnp.sum(jnp.where(down == across, log_sum, 0.0), axis=0, keepdims=True))
        osend[i] = jnp.where(head_lane == 0, outs[0], outs[1]).astype(BF16)
        slot = y * NY + wrap(y + rel, NY)
        lget[core, slot] = jnp.concatenate(sums, axis=0)
        oget[core, slot] = osend[i, pl.ds(pl.multiple_of(t * own, own), own), :]
        for k in (2, 1, 3, 0):
            for c in range(2):
                def go_to(c=c, k=k):
                    device = dev(dy=k, c=c)
                    rows = pl.ds(pl.multiple_of(device[1] * own, own), own)
                    rc(osend.at[i, rows], oget.at[core, slot], s_f.at[0], r_f.at[0], device).start()
                    rc(lget.at[core, slot], lget.at[core, slot], s_f.at[1], r_f.at[1], device).start()
                if k:
                    go_to()
                else:
                    pl.when(core != c)(go_to)

    order = (0, 1, 3, 2)
    groups = [(ref, h, rel) for rel in order for ref, h in ((kown, 0), (koth, 0), (kown, 1), (koth, 1))]
    events = {
        0: [lambda: queries_of(0)],
        1: [lambda: a_part(2)],
        3: [lambda: heads_in(1)],
        7: [lambda: heads_in(3)],
        11: [lambda: heads_in(2)],
        14: [wo_cross],
    }
    for j, (ref, h, rel) in enumerate(groups):
        for event in events.get(j, ()):
            event()
        if j == 1 or j == 3:
            got(koth.at[:, pl.ds(4 * h, 4)], r_d.at[h])
        expand(j)
        if j % 4 == 3 and j < 15:
            queries_of(groups[j + 1][2])
        if j >= 1:
            score(j - 1)
        if j >= 2:
            weigh(j - 2)
            if (j - 2) % 4 == 3:
                close((j - 2) // 4, groups[j - 2][2])
    last = len(groups) - 1
    score(last)
    weigh(last - 1)
    weigh(last)
    close(last // 4, groups[last][2])

    c_out.wait()
    got(lget.at[:, pl.ds(0, 14)], r_f.at[1])
    got(oget.at[:, pl.ds(0, 14)], r_f.at[0])
    spot = lax.broadcasted_iota(jnp.int32, (own, block), 0) + t * own
    spot = spot == lax.broadcasted_iota(jnp.int32, (own, block), 1)
    own_lane = lax.broadcasted_iota(jnp.int32, (own, nk), 1) // VDIM

    def column(row):
        return jnp.sum(jnp.where(spot, jnp.broadcast_to(row, (own, block)), 0.0), axis=-1, keepdims=True)

    got(wo.at[:, 0], r_wo.at[3])
    mixed = jnp.zeros((own, width), F32)
    for p in range(NY):
        merged = []
        for c in range(2):
            logs = [lget[c, q * NY + p] for q in range(NY)]
            most = jnp.maximum(jnp.maximum(logs[0], logs[1]), jnp.maximum(logs[2], logs[3]))
            shares = [jnp.exp2(log - most) for log in logs]
            whole = (shares[0] + shares[1]) + (shares[2] + shares[3])
            total = jnp.zeros((own, nk), F32)
            for q in range(NY):
                share = shares[q] / whole
                both = jnp.where(own_lane == 0, column(share[:1]), column(share[1:]))
                total = total + both * oget[c, q * NY + p].astype(F32)
            merged.append(total.astype(BF16))
        weights = jnp.concatenate([wo[p, c].reshape(width, nk) for c in range(2)], axis=1)
        mixed = mixed + dot_t(jnp.concatenate(merged, axis=1), weights)
    out[...] = rms(mixed.astype(BF16), gain_out[...])
    logs = [lget[core, q * NY + y] for q in range(NY)]
    most = jnp.maximum(jnp.maximum(logs[0], logs[1]), jnp.maximum(logs[2], logs[3]))
    shares = [jnp.exp2(log - most) for log in logs]
    whole = (shares[0] + shares[1]) + (shares[2] + shares[3])
    log_out[...] = most * math.log(2.0) + jnp.log(whole)

    for gather in (g_up, g_uq, g_wo):
        gather.drain()
    sent(up.at[pl.ds(0, 3)], s_up.at[2])
    sent(uq.at[pl.ds(0, 3)], s_uq.at[2])
    sent(wo.at[pl.ds(0, 3), core, 0, 0], s_wo.at[2])
    sent(wo.at[:, 0], s_wo.at[3])
    sent(tok.at[core], s_tok.at[0])
    sent(kown.at[pl.ds(0, 3)], s_a.at[0])
    sent(kown, s_d.at[0])
    sent(oget.at[:, pl.ds(0, 14)], s_f.at[0])
    sent(lget.at[:, pl.ds(0, 14)], s_f.at[1])

    @pl.when(core == 1)
    def _():
        g_k.drain()
        g_wr.drain()
        sent(kown.at[0, pl.ds(0, 7)], s_z.at[0])
        sent(kown.at[0], s_z.at[1])

    @pl.when(core == 0)
    def _():
        g_q.drain()
        sent(ql, s_q.at[1])
        sent(ql.at[pl.ds(0, 3)], s_q.at[0])


def on_device(n, ntp, tokens, doc_ids, down_q, down_k, down_r, gain_q, gain_k, up_q, up_k, up_v, out_w, gain_o):
    own, width = tokens.shape
    block = doc_ids.shape[0]
    heads = up_k.shape[1] // NOPE
    rank = down_k.shape[1]
    nq, nk, nv = up_q.shape[1], up_k.shape[1], up_v.shape[1]
    turn_in, turn_block, pick, pick_key, mix = tables(n, block, heads)
    vmem = pl.BlockSpec(memory_space=pltpu.VMEM)
    hbm = pl.BlockSpec(memory_space=pl.ANY)
    dma = lambda k: pltpu.SemaphoreType.DMA((k,))
    v = lambda *shape, dtype=BF16: pltpu.VMEM(shape, dtype)
    rows = heads * block
    scratch = [
        pltpu.VMEM((1, block), jnp.int32), v(1, rank, dtype=F32), v(1, width, dtype=F32), v(1, 256, dtype=F32), v(ROPE, 256),
        v(128, 128), v(2 * own, width), v(width // n, ROPE), v(width, 128),
        v(2, own, width), v(NZ, NX, width // n, rank), v(NZ, NX, width // n // 4, 128, dtype=F32),
        v(NY, NZ, NX, rank // n, nq), v(NY, NZ, NX, rank // n, nk + nv), v(NY, 2, NZ, NX, width // n, nv),
        v(NY, rank, nq), v(NY, rank, nk + nv), v(NY, 2 * own, rank),
        v(NX, NZ, 5, own // 2, 128), v(NX, NZ, 5, own // 2, 128), v(5, own // 2, 128),
        v(block, 256, dtype=F32), v(block, 128, dtype=F32), v(block, 128, dtype=F32), v(*pick.shape),
        v(NY, 2, rows, 256),
        v(2, 2, rows, 256, dtype=F32), v(2, 2, 256, nk), v(3, 512, nv),
        v(2, rows, 128, dtype=F32), v(2, rows, 128, dtype=F32), v(2, rows, 128, dtype=F32),
        v(NY, block, nv), v(2, NY * NY, own, nv), v(2, NY * NY, heads, block, dtype=F32),
        pltpu.SemaphoreType.REGULAR,
        dma(15), dma(1), dma(1), dma(2), dma(8), dma(2), dma(8), dma(3), dma(5), dma(3), dma(5), dma(4), dma(4),
        dma(2), dma(1), dma(1), dma(7), dma(2), dma(3), dma(1), dma(2), dma(2), dma(2),
    ]
    mixed, log_sums = pl.pallas_call(
        functools.partial(kernel, n, ntp, heads),
        out_shape=(
            jax.ShapeDtypeStruct((own, width), BF16),
            jax.ShapeDtypeStruct((heads, block), F32),
        ),
        in_specs=[hbm] * 17,
        out_specs=(vmem, vmem),
        scratch_shapes=scratch,
        compiler_params=pltpu.CompilerParams(
            collective_id=0, has_side_effects=True, vmem_limit_bytes=60 * 1024 * 1024
        ),
    )(
        tokens, doc_ids[None, :], down_q, down_k, down_r, gain_q[None, :], gain_k[None, :],
        up_q, up_k, up_v, out_w.T, gain_o[None, :],
        jnp.asarray(turn_in), jnp.asarray(turn_block[:, None, :]), jnp.asarray(pick, BF16), jnp.asarray(pick_key, BF16), jnp.asarray(mix, BF16),
    )
    return mixed, log_sums.T


def solution(mesh):
    assert mesh.shape["tp"] == 2 * NY and mesh.shape["sp"] == NX * NZ
    placed = (
        P(("sp", "tp"), None), P("sp"), P("sp", None), P("sp", None), P("sp", None), P(), P(),
        P("sp", "tp"), P("sp", "tp"), P("sp", "tp"), P("tp", "sp"), P(),
    )
    return jax.shard_map(
        functools.partial(on_device, mesh.shape["sp"], mesh.shape["tp"]),
        mesh=mesh,
        in_specs=placed,
        out_specs=(P(("sp", "tp"), None), P("sp", "tp")),
        check_vma=False,
    )
```

time: 59.7 us -> 60 us (level)
  no operation moved by 1% of the time
where the time goes in v4:
time: 60 us; the launch traced here: 59.9 us
  Pallas kernels  57.2 us (95%)
  local copies, waits for them, and re-layouts  2.06 us (3%)
  between operations  0.65 us (1%)
    pallas_call x1, Pallas kernels, on_device(): pl.pallas_call(functools.partial(kernel, n, ntp, heads), out_shape=(jax.S...  57.2 us
    unnamed x4, local copies, waits for them, and re-layouts  2.06 us

profile of v4, /device:TPU:1, one launch (start us, length us, event | category | flops | bytes accessed | tf_op | source)
XLA Modules:
  0.0 59.9 jit_solution(3476684321484603687)
XLA Ops:
  0.6 57.2 %shard_map.176 = (bf16[32,1024]{1,0:T(8,128)(2,1)}, f32[2,256]{1,0:T(2,128)}) custom-call(bf16[32,1024]{1,0:T(8,128)(2,1)} %tokens.1, s32[1,256]{1,0:T(1,128)} %bitcast.9, bf16[32,256]{1,0:T(8,128)(2,1)} %down_q.1, bf16[32,256]{1,0:T(8,128)(2,1)} %down_k.1, bf16[32,32]{1,0:T(8,128)(2,1)} %down_r.1, f32[1,256]{1,0:T(1,128)} %bitcast.10, f32[1,256]{1,0:T(1,128)} %bitcast.11, ...), custom_call_target="tpu_custom_call" | custom-call | tf_op jit(solution)/shard_map/pallas_call | solution.py:600
  57.8 0.0 copy-start
  57.8 1.5 %copy.21 = bf16[32,1024]{1,0:T(8,128)(2,1)} copy(bf16[32,1024]{1,0:T(8,128)(2,1)} %get-tuple-element.8) | data formatting | bytes 131072
  59.3 0.0 copy-done
  59.3 0.6 copy.22
Async XLA Ops:
  57.8 1.5 %copy-start = (f32[2,256]{1,0:T(2,128)S(1)}, f32[2,256]{1,0:T(2,128)}, u32[]{:S(2)}) copy-start(f32[2,256]{1,0:T(2,128)} %get-tuple-element.5) | copy-start | bytes 6148

commit v5 on v4

--- a/solution.py
+++ b/solution.py
@@ -217,22 +217,37 @@
     g_q = Gather(lambda i, j: w.at[i, j], s_w, r_w)
     g_uq = Gather(lambda i, j: uq.at[0, i, j], s_uq, r_uq)
     g_up = Gather(lambda i, j: up.at[0, i, j], s_up, r_up)
-    g_wo = Gather(lambda i, j: wo.at[:, core, i, j], s_wo, r_wo)
+    g_w0 = Gather(lambda i, j: wo.at[:, 0, i, j], s_wo, r_wo)
+    g_w1 = Gather(lambda i, j: wo.at[y, 1, i, j], s_wo, r_wo)
 
     def wo_y():
-        here = wo.at[y, core, z, x]
+        here = wo.at[y, 0, z, x]
         for k in (2, 1, 3):
             rc(here, here, s_wo.at[2], r_wo.at[2], dev(dy=k)).start()
 
     def wo_z():
-        got(wo.at[pl.ds(0, 3), core, z, x], r_wo.at[2])
-        g_wo.start_z()
+        got(wo.at[pl.ds(0, 3), 0, z, x], r_wo.at[2])
+        g_w0.start_z()
+
+    def wo_last():
+        pl.when(core == 0)(g_w0.start_x)
+
+        @pl.when(core == 1)
+        def _():
+            g_w1.finish()
+            here = wo.at[y, 1]
+            for k in (2, 1, 3):
+                rc(here, here, s_wo.at[2], r_wo.at[2], dev(dy=k)).start()
 
     def wo_cross():
-        g_wo.finish()
+        pl.when(core == 0)(g_w0.finish)
+
+        @pl.when(core == 1)
+        def _():
+            got(wo.at[pl.ds(0, 3), 1], r_wo.at[2])
+
         here = wo.at[:, core]
         rc(here, here, s_wo.at[3], r_wo.at[3], c_dev).start()
-
 
     def heads_y(ref, g, s, r):
         g.finish()
@@ -258,9 +273,9 @@
         g_k.pass_x(0)
         g_wr.pass_x(0)
         c_partner.start()
-        wo_y()
         g_up.start_z()
         g_uq.start_z()
+        g_w1.start_z()
         for d in NEAR[1:]:
             g_k.pass_x(d)
             g_wr.pass_x(d)
@@ -268,7 +283,7 @@
                 pl.semaphore_signal(go, inc=1, device_id=c_dev, device_id_type=MESH)
         g_up.start_x()
         g_uq.start_x()
-        wo_z()
+        g_w1.start_x()
         got(tok.at[1 - core], r_tok.at[0])
         both_tokens = tok[...].reshape(2 * own, width)
         for j in range(width // 128):
@@ -383,7 +398,6 @@
     z_part(1)
     z_part(2)
     a_part(1)
-    g_wo.start_x()
 
     @pl.when(core == 1)
     def _():
@@ -484,10 +498,10 @@
     events = {
         0: [lambda: queries_of(0)],
         1: [lambda: a_part(2)],
+        2: [wo_last],
         3: [lambda: heads_in(1)],
         7: [lambda: heads_in(3)],
         11: [lambda: heads_in(2)],
-        14: [wo_cross],
     }
     for j, (ref, h, rel) in enumerate(groups):
         for event in events.get(j, ()):
@@ -508,6 +522,7 @@
     weigh(last - 1)
     weigh(last)
     close(last // 4, groups[last][2])
+    wo_cross()
 
     c_out.wait()
     got(lget.at[:, pl.ds(0, 14)], r_f.at[1])
@@ -543,11 +558,10 @@
     whole = (shares[0] + shares[1]) + (shares[2] + shares[3])
     log_out[...] = most * math.log(2.0) + jnp.log(whole)
 
-    for gather in (g_up, g_uq, g_wo):
+    for gather in (g_up, g_uq):
         gather.drain()
     sent(up.at[pl.ds(0, 3)], s_up.at[2])
     sent(uq.at[pl.ds(0, 3)], s_uq.at[2])
-    sent(wo.at[pl.ds(0, 3), core, 0, 0], s_wo.at[2])
     sent(wo.at[:, 0], s_wo.at[3])
     sent(tok.at[core], s_tok.at[0])
     sent(kown.at[pl.ds(0, 3)], s_a.at[0])
@@ -559,12 +573,16 @@
     def _():
         g_k.drain()
         g_wr.drain()
+        g_w1.drain()
+        sent(wo.at[pl.ds(0, 3), 1], s_wo.at[2])
         sent(kown.at[0, pl.ds(0, 7)], s_z.at[0])
         sent(kown.at[0], s_z.at[1])
 
     @pl.when(core == 0)
     def _():
         g_q.drain()
+        g_w0.drain()
+        sent(wo.at[pl.ds(0, 3), 0, 0, 0], s_wo.at[2])
         sent(ql, s_q.at[1])
         sent(ql.at[pl.ds(0, 3)], s_q.at[0])
 

time: 60 us -> 55.7 us (0.928)
  Pallas kernels: 57.2 us -> 52.9 us
    pallas_call x1, Pallas kernels: 57.2 us -> 52.9 us  [on_device(): pl.pallas_call(functools.partial(kernel, n, ntp, heads), out_shape=(jax.S...]
where the time goes in v5:
time: 55.7 us; the launch traced here: 55.6 us
  Pallas kernels  52.9 us (95%)
  local copies, waits for them, and re-layouts  2.06 us (4%)
  between operations  0.65 us (1%)
    pallas_call x1, Pallas kernels, on_device(): pl.pallas_call(functools.partial(kernel, n, ntp, heads), out_shape=(jax.S...  52.9 us
    unnamed x4, local copies, waits for them, and re-layouts  2.06 us

profile of v5, /device:TPU:1, one launch (start us, length us, event | category | flops | bytes accessed | tf_op | source)
XLA Modules:
  0.0 55.6 jit_solution(11988750012541166408)
XLA Ops:
  0.6 52.9 %shard_map.176 = (bf16[32,1024]{1,0:T(8,128)(2,1)}, f32[2,256]{1,0:T(2,128)}) custom-call(bf16[32,1024]{1,0:T(8,128)(2,1)} %tokens.1, s32[1,256]{1,0:T(1,128)} %bitcast.9, bf16[32,256]{1,0:T(8,128)(2,1)} %down_q.1, bf16[32,256]{1,0:T(8,128)(2,1)} %down_k.1, bf16[32,32]{1,0:T(8,128)(2,1)} %down_r.1, f32[1,256]{1,0:T(1,128)} %bitcast.10, f32[1,256]{1,0:T(1,128)} %bitcast.11, ...), custom_call_target="tpu_custom_call" | custom-call | tf_op jit(solution)/shard_map/pallas_call | solution.py:618
  53.5 0.0 copy-start
  53.5 1.5 %copy.21 = bf16[32,1024]{1,0:T(8,128)(2,1)} copy(bf16[32,1024]{1,0:T(8,128)(2,1)} %get-tuple-element.8) | data formatting | bytes 131072
  55.0 0.0 copy-done
  55.0 0.6 %copy.22 = f32[256,2]{0,1:T(2,128)} copy(f32[256,2]{0,1:T(2,128)S(1)} %bitcast.8) | data formatting | bytes 4096
Async XLA Ops:
  53.5 1.5 %copy-start = (f32[2,256]{1,0:T(2,128)S(1)}, f32[2,256]{1,0:T(2,128)}, u32[]{:S(2)}) copy-start(f32[2,256]{1,0:T(2,128)} %get-tuple-element.5) | copy-start | bytes 6148

commit v6 on v5

--- a/solution.py
+++ b/solution.py
@@ -249,11 +249,11 @@
         here = wo.at[:, core]
         rc(here, here, s_wo.at[3], r_wo.at[3], c_dev).start()
 
-    def heads_y(ref, g, s, r):
-        g.finish()
-        for k in (1, 3, 2):
+    def heads_y(steps):
+        for k in steps:
             rel = -k % NY
-            rc(ref.at[0], ref.at[rel], s.at[2], r.at[1 + rel], dev(dy=k)).start()
+            rc(up.at[0], up.at[rel], s_up.at[2], r_up.at[1 + rel], dev(dy=k)).start()
+            rc(uq.at[0], uq.at[rel], s_uq.at[2], r_uq.at[1 + rel], dev(dy=k)).start()
 
     def heads_in(rel):
         if rel:
@@ -279,11 +279,10 @@
         for d in NEAR[1:]:
             g_k.pass_x(d)
             g_wr.pass_x(d)
-            if d == 6:
+            if d == 1:
                 pl.semaphore_signal(go, inc=1, device_id=c_dev, device_id_type=MESH)
         g_up.start_x()
         g_uq.start_x()
-        g_w1.start_x()
         got(tok.at[1 - core], r_tok.at[0])
         both_tokens = tok[...].reshape(2 * own, width)
         for j in range(width // 128):
@@ -305,9 +304,9 @@
         g_uq.start_z()
         pl.semaphore_wait(go, 1)
         g_q.start_z()
+        g_q.start_x()
         g_up.start_x()
         g_uq.start_x()
-        g_q.start_x()
         wo_z()
 
     def project():
@@ -338,11 +337,11 @@
                     ks[i] = tile
         here = kown.at[0, 0]
         rc(ks, here, s_z.at[1], r_z.at[2], dev(c=0)).start()
+        for k in (2, 1, 3):
+            rc(here, kown.at[-k % NX, 0], s_a.at[0], r_a.at[0], dev(dx=k)).start()
         for d in (4, 1, 7, 6, 2, 3, 5):
             pos = ZPOS[-d % NZ]
-            there, sem = kown.at[0, pos], r_z.at[0 if pos < 4 else 1]
-            rc(ks, there, s_z.at[1], sem, dev(dz=d, c=0)).start()
-            rc(here, there, s_z.at[0], sem, dev(dz=d)).start()
+            rc(ks, kown.at[0, pos], s_z.at[1], r_z.at[0 if pos < 4 else 1], dev(dz=d, c=0)).start()
 
     parts = ((0, 1), (1, 3), (4, 4))
 
@@ -361,9 +360,7 @@
 
     def z_part(p):
         if p == 0:
-            @pl.when(core == 0)
-            def _():
-                got(kown.at[0, 0], r_z.at[2])
+            got(kown.at[0, 0], r_z.at[2])
         else:
             got(kown.at[0, pl.ds(*parts[p])], r_z.at[p - 1])
         a_send(p)
@@ -378,10 +375,15 @@
                 got(kown.at[rel, pl.ds(*parts[p])], r_a.at[3 * p - 3 + rel])
                 cross(rel, 1, p)
 
-    z_part(0)
+    def rows_of(h):
+        cut = pl.ds(1, 3) if h == 0 else pl.ds(4, 4)
+        got(kown.at[:, cut], r_z.at[h])
+        cut = pl.ds(4 * h, 4)
+        rc(kown.at[:, cut], koth.at[:, cut], s_d.at[0], r_d.at[h], c_dev).start()
 
     @pl.when(core == 0)
     def _():
+        z_part(0)
         got(tok.at[1 - core], r_tok.at[0])
         g_q.finish()
         ql[y] = project()
@@ -390,14 +392,35 @@
             for c in range(2):
                 rc(here, here, s_q.at[c], r_q.at[0], dev(dy=k, c=c)).start()
         rc(here, here, s_q.at[1], r_q.at[0], dev(c=1)).start()
-
-    heads_y(up, g_up, s_up, r_up)
-    heads_y(uq, g_uq, s_uq, r_uq)
+        g_up.finish()
+        g_uq.finish()
+        heads_y((1, 3))
+        a_part(0)
+        z_part(1)
+        z_part(2)
+        heads_y((2,))
+
+    @pl.when(core == 1)
+    def _():
+        g_up.finish()
+        g_uq.finish()
+        heads_y((1, 3))
+        got(kown.at[pl.ds(1, 3), 0], r_a.at[0])
+        for d in (1, 7, 6, 4, 3, 5, 2):
+            pos = ZPOS[-d % NZ]
+            rc(kown.at[:, 0], kown.at[:, pos], s_z.at[0], r_z.at[0 if pos < 4 else 1], dev(dz=d)).start()
+        g_w1.start_x()
+
     heads_in(0)
-    a_part(0)
-    z_part(1)
-    z_part(2)
-    a_part(1)
+
+    @pl.when(core == 0)
+    def _():
+        a_part(1)
+
+    @pl.when(core == 1)
+    def _():
+        rows_of(0)
+        heads_y((2,))
 
     @pl.when(core == 1)
     def _():
@@ -495,11 +518,15 @@
 
     order = (0, 1, 3, 2)
     groups = [(ref, h, rel) for rel in order for ref, h in ((kown, 0), (koth, 0), (kown, 1), (koth, 1))]
+    def second_half():
+        pl.when(core == 0)(lambda: a_part(2))
+        pl.when(core == 1)(lambda: rows_of(1))
+
     events = {
         0: [lambda: queries_of(0)],
-        1: [lambda: a_part(2)],
-        2: [wo_last],
+        2: [second_half],
         3: [lambda: heads_in(1)],
+        4: [wo_last],
         7: [lambda: heads_in(3)],
         11: [lambda: heads_in(2)],
     }
@@ -564,7 +591,6 @@
     sent(uq.at[pl.ds(0, 3)], s_uq.at[2])
     sent(wo.at[:, 0], s_wo.at[3])
     sent(tok.at[core], s_tok.at[0])
-    sent(kown.at[pl.ds(0, 3)], s_a.at[0])
     sent(kown, s_d.at[0])
     sent(oget.at[:, pl.ds(0, 14)], s_f.at[0])
     sent(lget.at[:, pl.ds(0, 14)], s_f.at[1])
@@ -575,13 +601,15 @@
         g_wr.drain()
         g_w1.drain()
         sent(wo.at[pl.ds(0, 3), 1], s_wo.at[2])
-        sent(kown.at[0, pl.ds(0, 7)], s_z.at[0])
+        sent(kown.at[:, pl.ds(0, 7)], s_z.at[0])
         sent(kown.at[0], s_z.at[1])
+        sent(kown.at[pl.ds(0, 3), 0], s_a.at[0])
 
     @pl.when(core == 0)
     def _():
         g_q.drain()
         g_w0.drain()
+        sent(kown.at[pl.ds(0, 3)], s_a.at[0])
         sent(wo.at[pl.ds(0, 3), 0, 0, 0], s_wo.at[2])
         sent(ql, s_q.at[1])
         sent(ql.at[pl.ds(0, 3)], s_q.at[0])

time: 55.7 us -> 55.1 us (0.989)
  Pallas kernels: 52.9 us -> 52.2 us
    pallas_call x1, Pallas kernels: 52.9 us -> 52.2 us  [on_device(): pl.pallas_call(functools.partial(kernel, n, ntp, heads), out_shape=(jax.S...]
where the time goes in v6:
time: 55.1 us; the launch traced here: 54.9 us
  Pallas kernels  52.2 us (95%)
  local copies, waits for them, and re-layouts  2.06 us (4%)
  between operations  0.65 us (1%)
    pallas_call x1, Pallas kernels, on_device(): pl.pallas_call(functools.partial(kernel, n, ntp, heads), out_shape=(jax.S...  52.2 us
    unnamed x4, local copies, waits for them, and re-layouts  2.06 us

profile of v6, /device:TPU:1, one launch (start us, length us, event | category | flops | bytes accessed | tf_op | source)
XLA Modules:
  0.0 54.9 jit_solution(1567017710727868383)
XLA Ops:
  0.6 52.2 %shard_map.176 = (bf16[32,1024]{1,0:T(8,128)(2,1)}, f32[2,256]{1,0:T(2,128)}) custom-call(bf16[32,1024]{1,0:T(8,128)(2,1)} %tokens.1, s32[1,256]{1,0:T(1,128)} %bitcast.9, bf16[32,256]{1,0:T(8,128)(2,1)} %down_q.1, bf16[32,256]{1,0:T(8,128)(2,1)} %down_k.1, bf16[32,32]{1,0:T(8,128)(2,1)} %down_r.1, f32[1,256]{1,0:T(1,128)} %bitcast.10, f32[1,256]{1,0:T(1,128)} %bitcast.11, ...), custom_call_target="tpu_custom_call" | custom-call | tf_op jit(solution)/shard_map/pallas_call | solution.py:646
  52.9 0.0 copy-start
  52.9 1.5 %copy.21 = bf16[32,1024]{1,0:T(8,128)(2,1)} copy(bf16[32,1024]{1,0:T(8,128)(2,1)} %get-tuple-element.8) | data formatting | bytes 131072
  54.4 0.0 copy-done
  54.4 0.6 %copy.22 = f32[256,2]{0,1:T(2,128)} copy(f32[256,2]{0,1:T(2,128)S(1)} %bitcast.8) | data formatting | bytes 4096
Async XLA Ops:
  52.9 1.5 %copy-start = (f32[2,256]{1,0:T(2,128)S(1)}, f32[2,256]{1,0:T(2,128)}, u32[]{:S(2)}) copy-start(f32[2,256]{1,0:T(2,128)} %get-tuple-element.5) | copy-start | bytes 6148

commit v7 on v6

--- a/solution.py
+++ b/solution.py
@@ -230,24 +230,55 @@
         g_w0.start_z()
 
     def wo_last():
-        pl.when(core == 0)(g_w0.start_x)
+        @pl.when(core == 0)
+        def _():
+            got(wo.at[:, 0, pl.ds(0, NZ - 1), x], r_wo.at[0])
+            here = wo.at[:, 0, :, x]
+            rc(here, here, s_wo.at[1], r_wo.at[4], dev(dx=1)).start()
+            rc(here, here, s_wo.at[1], r_wo.at[5], dev(dx=-1)).start()
+            rc(here, here, s_wo.at[3], r_wo.at[3], c_dev).start()
 
         @pl.when(core == 1)
         def _():
             g_w1.finish()
             here = wo.at[y, 1]
-            for k in (2, 1, 3):
-                rc(here, here, s_wo.at[2], r_wo.at[2], dev(dy=k)).start()
-
-    def wo_cross():
-        pl.when(core == 0)(g_w0.finish)
+            rc(here, here, s_wo.at[2], r_wo.at[4], dev(dy=1)).start()
+            rc(here, here, s_wo.at[2], r_wo.at[5], dev(dy=-1)).start()
+            rc(here, here, s_wo.at[3], r_wo.at[3], c_dev).start()
+
+    def wo_far():
+        low, high = pl.ds(0, NZ // 2), pl.ds(NZ // 2, NZ // 2)
+
+        @pl.when(core == 0)
+        def _():
+            for d, cut, sem in ((-1, low, 4), (1, high, 5)):
+                whole = wo.at[:, 0, :, wrap(x + d, NX)]
+                part = wo.at[:, 0, cut, wrap(x + d, NX)]
+                got(whole, r_wo.at[sem])
+                rc(part, part, s_wo.at[1], r_wo.at[1], dev(dx=-d)).start()
+                rc(whole, whole, s_wo.at[3], r_wo.at[3], c_dev).start()
 
         @pl.when(core == 1)
         def _():
-            got(wo.at[pl.ds(0, 3), 1], r_wo.at[2])
-
-        here = wo.at[:, core]
-        rc(here, here, s_wo.at[3], r_wo.at[3], c_dev).start()
+            for d, cut, sem in ((-1, low, 4), (1, high, 5)):
+                whole = wo.at[wrap(y + d, NY), 1]
+                part = wo.at[wrap(y + d, NY), 1, cut]
+                got(whole, r_wo.at[sem])
+                rc(part, part, s_wo.at[2], r_wo.at[2], dev(dy=-d)).start()
+                rc(whole, whole, s_wo.at[3], r_wo.at[3], c_dev).start()
+
+    def wo_cross():
+        @pl.when(core == 0)
+        def _():
+            here = wo.at[:, 0, :, wrap(x + 2, NX)]
+            got(here, r_wo.at[1])
+            rc(here, here, s_wo.at[3], r_wo.at[3], c_dev).start()
+
+        @pl.when(core == 1)
+        def _():
+            here = wo.at[wrap(y + 2, NY), 1]
+            got(here, r_wo.at[2])
+            rc(here, here, s_wo.at[3], r_wo.at[3], c_dev).start()
 
     def heads_y(steps):
         for k in steps:
@@ -255,10 +286,16 @@
             rc(up.at[0], up.at[rel], s_up.at[2], r_up.at[1 + rel], dev(dy=k)).start()
             rc(uq.at[0], uq.at[rel], s_uq.at[2], r_uq.at[1 + rel], dev(dy=k)).start()
 
+    def heads_far(rel):
+        got(up.at[rel], r_up.at[1 + rel])
+        got(uq.at[rel], r_uq.at[1 + rel])
+        if rel != 2:
+            cut = pl.ds(0 if rel == 3 else NZ // 2, NZ // 2)
+            device = dev(dy=1 if rel == 3 else -1)
+            rc(up.at[rel, cut], up.at[2, cut], s_up.at[2], r_up.at[3], device).start()
+            rc(uq.at[rel, cut], uq.at[2, cut], s_uq.at[2], r_uq.at[3], device).start()
+
     def heads_in(rel):
-        if rel:
-            got(up.at[rel], r_up.at[1 + rel])
-            got(uq.at[rel], r_uq.at[1 + rel])
         for j in range(n):
             up_flat[rel, j * 8 : (j + 1) * 8, :] = up[rel, j // NX, j % NX]
             uq_flat[rel, j * 8 : (j + 1) * 8, :] = uq[rel, j // NX, j % NX]
@@ -385,6 +422,7 @@
     def _():
         z_part(0)
         got(tok.at[1 - core], r_tok.at[0])
+        z_part(1)
         g_q.finish()
         ql[y] = project()
         here = ql.at[y]
@@ -392,13 +430,11 @@
             for c in range(2):
                 rc(here, here, s_q.at[c], r_q.at[0], dev(dy=k, c=c)).start()
         rc(here, here, s_q.at[1], r_q.at[0], dev(c=1)).start()
+        z_part(2)
         g_up.finish()
         g_uq.finish()
         heads_y((1, 3))
         a_part(0)
-        z_part(1)
-        z_part(2)
-        heads_y((2,))
 
     @pl.when(core == 1)
     def _():
@@ -420,7 +456,6 @@
     @pl.when(core == 1)
     def _():
         rows_of(0)
-        heads_y((2,))
 
     @pl.when(core == 1)
     def _():
@@ -524,11 +559,11 @@
 
     events = {
         0: [lambda: queries_of(0)],
-        2: [second_half],
-        3: [lambda: heads_in(1)],
-        4: [wo_last],
+        2: [second_half, lambda: heads_far(1), lambda: heads_far(3)],
+        3: [lambda: heads_in(1), wo_last],
         7: [lambda: heads_in(3)],
-        11: [lambda: heads_in(2)],
+        11: [lambda: heads_far(2), lambda: heads_in(2)],
+        14: [wo_far],
     }
     for j, (ref, h, rel) in enumerate(groups):
         for event in events.get(j, ()):
@@ -640,7 +675,7 @@
         v(2, rows, 128, dtype=F32), v(2, rows, 128, dtype=F32), v(2, rows, 128, dtype=F32),
         v(NY, block, nv), v(2, NY * NY, own, nv), v(2, NY * NY, heads, block, dtype=F32),
         pltpu.SemaphoreType.REGULAR,
-        dma(15), dma(1), dma(1), dma(2), dma(8), dma(2), dma(8), dma(3), dma(5), dma(3), dma(5), dma(4), dma(4),
+        dma(15), dma(1), dma(1), dma(2), dma(8), dma(2), dma(8), dma(3), dma(5), dma(3), dma(5), dma(4), dma(6),
         dma(2), dma(1), dma(1), dma(7), dma(2), dma(3), dma(1), dma(2), dma(2), dma(2),
     ]
     mixed, log_sums = pl.pallas_call(

time: 55.1 us -> 54 us (0.980)
  Pallas kernels: 52.2 us -> 51.1 us
    pallas_call x1, Pallas kernels: 52.2 us -> 51.1 us  [on_device(): pl.pallas_call(functools.partial(kernel, n, ntp, heads), out_shape=(jax.S...]
where the time goes in v7:
time: 54 us; the launch traced here: 53.8 us
  Pallas kernels  51.1 us (95%)
  local copies, waits for them, and re-layouts  2.06 us (4%)
  between operations  0.65 us (1%)
    pallas_call x1, Pallas kernels, on_device(): pl.pallas_call(functools.partial(kernel, n, ntp, heads), out_shape=(jax.S...  51.1 us
    unnamed x4, local copies, waits for them, and re-layouts  2.06 us

profile of v7, /device:TPU:1, one launch (start us, length us, event | category | flops | bytes accessed | tf_op | source)
XLA Modules:
  0.0 53.8 jit_solution(7509174385857658554)
XLA Ops:
  0.6 51.1 %shard_map.176 = (bf16[32,1024]{1,0:T(8,128)(2,1)}, f32[2,256]{1,0:T(2,128)}) custom-call(bf16[32,1024]{1,0:T(8,128)(2,1)} %tokens.1, s32[1,256]{1,0:T(1,128)} %bitcast.9, bf16[32,256]{1,0:T(8,128)(2,1)} %down_q.1, bf16[32,256]{1,0:T(8,128)(2,1)} %down_k.1, bf16[32,32]{1,0:T(8,128)(2,1)} %down_r.1, f32[1,256]{1,0:T(1,128)} %bitcast.10, f32[1,256]{1,0:T(1,128)} %bitcast.11, ...), custom_call_target="tpu_custom_call" | custom-call | tf_op jit(solution)/shard_map/pallas_call | solution.py:681
  51.7 0.0 copy-start
  51.8 1.5 %copy.21 = bf16[32,1024]{1,0:T(8,128)(2,1)} copy(bf16[32,1024]{1,0:T(8,128)(2,1)} %get-tuple-element.8) | data formatting | bytes 131072
  53.2 0.0 copy-done
  53.2 0.6 %copy.22 = f32[256,2]{0,1:T(2,128)} copy(f32[256,2]{0,1:T(2,128)S(1)} %bitcast.8) | data formatting | bytes 4096
Async XLA Ops:
  51.7 1.5 %copy-start = (f32[2,256]{1,0:T(2,128)S(1)}, f32[2,256]{1,0:T(2,128)}, u32[]{:S(2)}) copy-start(f32[2,256]{1,0:T(2,128)} %get-tuple-element.5) | copy-start | bytes 6148

commit v8 on v7

--- a/solution.py
+++ b/solution.py
@@ -312,12 +312,12 @@
         c_partner.start()
         g_up.start_z()
         g_uq.start_z()
-        g_w1.start_z()
         for d in NEAR[1:]:
             g_k.pass_x(d)
             g_wr.pass_x(d)
             if d == 1:
                 pl.semaphore_signal(go, inc=1, device_id=c_dev, device_id_type=MESH)
+        g_w1.start_z()
         g_up.start_x()
         g_uq.start_x()
         got(tok.at[1 - core], r_tok.at[0])

time: 54 us -> 53.7 us (level)
  no operation moved by 1% of the time
where the time goes in v8:
time: 53.7 us; the launch traced here: 53.5 us
  Pallas kernels  50.8 us (95%)
  local copies, waits for them, and re-layouts  2.06 us (4%)
  between operations  0.65 us (1%)
    pallas_call x1, Pallas kernels, on_device(): pl.pallas_call(functools.partial(kernel, n, ntp, heads), out_shape=(jax.S...  50.8 us
    unnamed x4, local copies, waits for them, and re-layouts  2.06 us

profile of v8, /device:TPU:1, one launch (start us, length us, event | category | flops | bytes accessed | tf_op | source)
XLA Modules:
  0.0 53.5 jit_solution(10763317734040285312)
XLA Ops:
  0.6 50.8 %shard_map.176 = (bf16[32,1024]{1,0:T(8,128)(2,1)}, f32[2,256]{1,0:T(2,128)}) custom-call(bf16[32,1024]{1,0:T(8,128)(2,1)} %tokens.1, s32[1,256]{1,0:T(1,128)} %bitcast.9, bf16[32,256]{1,0:T(8,128)(2,1)} %down_q.1, bf16[32,256]{1,0:T(8,128)(2,1)} %down_k.1, bf16[32,32]{1,0:T(8,128)(2,1)} %down_r.1, f32[1,256]{1,0:T(1,128)} %bitcast.10, f32[1,256]{1,0:T(1,128)} %bitcast.11, ...), custom_call_target="tpu_custom_call" | custom-call | tf_op jit(solution)/shard_map/pallas_call | solution.py:681
  51.5 0.0 copy-start
  51.5 1.5 %copy.21 = bf16[32,1024]{1,0:T(8,128)(2,1)} copy(bf16[32,1024]{1,0:T(8,128)(2,1)} %get-tuple-element.8) | data formatting | bytes 131072
  52.9 0.0 copy-done
  52.9 0.6 %copy.22 = f32[256,2]{0,1:T(2,128)} copy(f32[256,2]{0,1:T(2,128)S(1)} %bitcast.8) | data formatting | bytes 4096
Async XLA Ops:
  51.5 1.5 %copy-start = (f32[2,256]{1,0:T(2,128)S(1)}, f32[2,256]{1,0:T(2,128)}, u32[]{:S(2)}) copy-start(f32[2,256]{1,0:T(2,128)} %get-tuple-element.5) | copy-start | bytes 6148

commit v9 on v8

--- a/solution.py
+++ b/solution.py
@@ -280,11 +280,11 @@
             got(here, r_wo.at[2])
             rc(here, here, s_wo.at[3], r_wo.at[3], c_dev).start()
 
-    def heads_y(steps):
-        for k in steps:
+    def heads_y(g, ref, s, r):
+        g.finish()
+        for k in (1, 3):
             rel = -k % NY
-            rc(up.at[0], up.at[rel], s_up.at[2], r_up.at[1 + rel], dev(dy=k)).start()
-            rc(uq.at[0], uq.at[rel], s_uq.at[2], r_uq.at[1 + rel], dev(dy=k)).start()
+            rc(ref.at[0], ref.at[rel], s.at[2], r.at[1 + rel], dev(dy=k)).start()
 
     def heads_far(rel):
         got(up.at[rel], r_up.at[1 + rel])
@@ -431,16 +431,14 @@
                 rc(here, here, s_q.at[c], r_q.at[0], dev(dy=k, c=c)).start()
         rc(here, here, s_q.at[1], r_q.at[0], dev(c=1)).start()
         z_part(2)
-        g_up.finish()
-        g_uq.finish()
-        heads_y((1, 3))
+        heads_y(g_up, up, s_up, r_up)
+        heads_y(g_uq, uq, s_uq, r_uq)
         a_part(0)
 
     @pl.when(core == 1)
     def _():
-        g_up.finish()
-        g_uq.finish()
-        heads_y((1, 3))
+        heads_y(g_up, up, s_up, r_up)
+        heads_y(g_uq, uq, s_uq, r_uq)
         got(kown.at[pl.ds(1, 3), 0], r_a.at[0])
         for d in (1, 7, 6, 4, 3, 5, 2):
             pos = ZPOS[-d % NZ]

time: 53.7 us -> 53.2 us (level)
  no operation moved by 1% of the time
where the time goes in v9:
time: 53.2 us; the launch traced here: 53.1 us
  Pallas kernels  50.4 us (95%)
  local copies, waits for them, and re-layouts  2.06 us (4%)
  between operations  0.65 us (1%)
    pallas_call x1, Pallas kernels, on_device(): pl.pallas_call(functools.partial(kernel, n, ntp, heads), out_shape=(jax.S...  50.4 us
    unnamed x4, local copies, waits for them, and re-layouts  2.06 us

profile of v9, /device:TPU:1, one launch (start us, length us, event | category | flops | bytes accessed | tf_op | source)
XLA Modules:
  0.0 53.1 jit_solution(5377980145915334554)
XLA Ops:
  0.6 50.4 %shard_map.176 = (bf16[32,1024]{1,0:T(8,128)(2,1)}, f32[2,256]{1,0:T(2,128)}) custom-call(bf16[32,1024]{1,0:T(8,128)(2,1)} %tokens.1, s32[1,256]{1,0:T(1,128)} %bitcast.9, bf16[32,256]{1,0:T(8,128)(2,1)} %down_q.1, bf16[32,256]{1,0:T(8,128)(2,1)} %down_k.1, bf16[32,32]{1,0:T(8,128)(2,1)} %down_r.1, f32[1,256]{1,0:T(1,128)} %bitcast.10, f32[1,256]{1,0:T(1,128)} %bitcast.11, ...), custom_call_target="tpu_custom_call" | custom-call | tf_op jit(solution)/shard_map/pallas_call | solution.py:679
  51.0 0.0 copy-start
  51.0 1.5 %copy.21 = bf16[32,1024]{1,0:T(8,128)(2,1)} copy(bf16[32,1024]{1,0:T(8,128)(2,1)} %get-tuple-element.8) | data formatting | bytes 131072
  52.5 0.0 copy-done
  52.5 0.6 %copy.22 = f32[256,2]{0,1:T(2,128)} copy(f32[256,2]{0,1:T(2,128)S(1)} %bitcast.8) | data formatting | bytes 4096
Async XLA Ops:
  51.0 1.5 %copy-start = (f32[2,256]{1,0:T(2,128)S(1)}, f32[2,256]{1,0:T(2,128)}, u32[]{:S(2)}) copy-start(f32[2,256]{1,0:T(2,128)} %get-tuple-element.5) | copy-start | bytes 6148
